TPU v7x, 32 devices: a whole 2x2x4 slice. The times are simulated.
32 devices in a mesh: gr: 2 (over x), fs: 4 (over z), tp: 4 (over y, core).
Axes of the slice: x: 2, y: 2, z: 4, core: 2. Of those that a mesh axis runs over, the one named last changes fastest.
Arguments:
- tokens: bfloat16 [4096, 2048], P(('gr', 'fs')), may hold values from -6 to 6
- routes: int32 [4096, 2], P(('gr', 'fs')), may hold values from 0 to 3, all different within a row; in each aligned block of 512 rows (0 to 511, 512 to 1023, ...) at most 384 rows name the same one
- route_weight: float32 [4096, 2], P(('gr', 'fs')), may hold values from 0.2 to 1
- gain: float32 [2048], P(('gr', 'fs')), may hold values from 0.1 to 1.9
- w_gate: bfloat16 [4, 2048, 4096], P(None, ('gr', 'fs'), 'tp'), may hold values from -0.125 to 0.125
- w_up: bfloat16 [4, 2048, 4096], P(None, ('gr', 'fs'), 'tp'), may hold values from -0.125 to 0.125
- w_down: bfloat16 [4, 2048, 4096], P(None, ('gr', 'fs'), 'tp'), may hold values from -0.09375 to 0.09375
Outputs:
- gate_out: bfloat16 [4, 2048, 4096], P('fs', None, 'tp')
- up_out: bfloat16 [4, 2048, 4096], P('fs', None, 'tp')
- down_out: bfloat16 [4, 2048, 4096], P('fs', None, 'tp')
- mixed: bfloat16 [4096, 2048], P(('gr', 'fs'), 'tp')
Inputs may be any that keep to these rules, and one draw needn't show every extreme that they name: `routes`: each row names two different experts. Among the 512 rows of one device no expert is named more than 384 times, and in every draw some device names some expert exactly 384 times.
All inputs are finite; a program needn't handle non-finite values.
Results may differ from a plain program's by a relative error of at most 0.015.
Values may be sent and summed in bfloat16 or wider, within the bound.
A program may use at most 128 MiB of HBM per device.

v0:
```python
import functools
import jax
import jax.numpy as jnp
from jax import lax
from jax.experimental import pallas as pl
from jax.experimental.pallas import tpu as pltpu
from jax.sharding import PartitionSpec as P

MESH = pl.DeviceIdType.MESH
VMEM_LIMIT = 66 * 1000 * 1000
EPSILON = 1e-05


def kernel(ng, nz, nt, tok_in, wt, gw, uw, dw, gout, uout, dout, mixed,
           tok, hid, part, crx, yrx, ret,
           ts, tr, fs_s, fr, own, ws, wr, xs, xr, cs, cr, ys, yr, rs, rr):
    g, z, t = lax.axis_index("gr"), lax.axis_index("fs"), lax.axis_index("tp")
    core, y = lax.rem(t, 2), lax.div(t, 2)
    rows, quarter = tok_in.shape[0], tok_in.shape[1] // nt
    chunk, width = gw.shape[1], gw.shape[2]
    chunks = ng * nz
    per_owner = chunks // nt
    srcs = (gw, uw, dw)
    outs = (gout, uout, dout)
    ks = sorted(range(1, nz), key=lambda k: min(k, nz - k))

    def to(k):
        return lax.rem(z + k, nz)

    def frm(k):
        return lax.rem(z + nz - k, nz)

    def rdma(src, dst, ss, rsem, dev):
        return pltpu.make_async_remote_copy(
            src_ref=src, dst_ref=dst, send_sem=ss, recv_sem=rsem, device_id=dev, device_id_type=MESH
        )

    def rows_of(m, group, zs):
        return outs[m].at[pl.ds(pl.multiple_of((group * nz + zs) * chunk, chunk), chunk), :]

    barrier = pltpu.get_barrier_semaphore()
    for k in range(1, nz):
        pl.semaphore_signal(barrier, inc=1, device_id={"fs": to(k)}, device_id_type=MESH)
    for j in range(1, nt):
        pl.semaphore_signal(barrier, inc=1, device_id={"tp": lax.rem(t + j, nt)}, device_id_type=MESH)
    pl.semaphore_signal(barrier, inc=1, device_id={"gr": 1 - g}, device_id_type=MESH)
    pl.semaphore_wait(barrier, nz + nt - 1)

    sends = []

    def z_send(m, k):
        c = rdma(srcs[m].at[to(k)], rows_of(m, g, z), ws.at[m, k], wr.at[m, k], {"fs": to(k)})
        c.start()
        sends.append(c)

    def x_send(m, k, src):
        c = rdma(src, rows_of(m, g, frm(k)), xs.at[m, k], xr.at[m, k], {"gr": 1 - g})
        c.start()
        sends.append(c)

    def z_take(m, k):
        ref = rows_of(m, g, frm(k))
        rdma(ref, ref, ws.at[m, k], wr.at[m, k], {"fs": to(k)}).wait_recv()
        x_send(m, k, ref)

    def x_take(m, k):
        ref = rows_of(m, 1 - g, frm(k))
        rdma(ref, ref, xs.at[m, k], xr.at[m, k], {"gr": 1 - g}).wait_recv()

    x_send(0, 0, gw.at[z])
    for k in ks:
        z_send(0, k)
    x_send(1, 0, uw.at[z])
    x_send(2, 0, dw.at[z])
    own_rows = pl.ds(pl.multiple_of((g * nz + z) * chunk, chunk), chunk)
    own_down = pltpu.make_async_copy(dw.at[z], dout.at[own_rows, :], own)
    own_down.start()

    step = 64

    @pl.loop(0, rows // step)
    def _(i):
        at = pl.ds(pl.multiple_of(i * step, step), step)
        x = tok_in[at, :].astype(jnp.float32)
        scale = lax.rsqrt(jnp.mean(x * x, axis=-1, keepdims=True) + EPSILON)
        x = (x * scale).astype(jnp.bfloat16)
        for q in range(nt):
            tok[q, z, at, :] = x[:, q * quarter:(q + 1) * quarter]

    for m in range(2):
        outs[m][own_rows, :] = srcs[m][z]

    guarded = []

    def guard(flag, c):
        @pl.when(flag)
        def _():
            c.start()
        guarded.append((flag, c))

    def hop(way, h, src):
        nxt = lax.rem(z + way + nz, nz)
        ref = tok.at[t, src]
        return rdma(ref, ref, ts.at[(way + 1) // 2, h], tr.at[src], {"fs": nxt})

    right, left = z + 1 < nz, z >= 1
    guard(right, hop(1, 0, z))
    guard(left, hop(-1, 0, z))
    z_send(1, ks[0])
    for k in ks:
        z_take(0, k)
    mate, over = y * 2 + 1 - core, (1 - y) * 2 + core
    for h in range(1, nz):
        for way in (1, -1):
            src = lax.rem(z - way * h + nz, nz)
            valid = z >= h if way == 1 else z + h < nz
            more = right if way == 1 else left
            ref = tok.at[t, src]

            @pl.when(valid)
            def _(ref=ref, src=src):
                rdma(ref, ref, ts.at[0, 0], tr.at[src], {"fs": lax.rem(z + 1, nz)}).wait_recv()
            guard(jnp.logical_and(valid, more), hop(way, h, src))
            guard(valid, rdma(ref, ref, fs_s.at[1, src], fr.at[1, src], {"tp": over}))
            guard(valid, rdma(ref, ref, fs_s.at[0, src], fr.at[0, src], {"tp": mate}))
        if h < len(ks):
            z_send(1, ks[h])
    for k in ks:
        z_send(2, k)
    z_take(1, ks[0])
    for k in ks:
        src = frm(k)
        ref = tok.at[over, src]
        rdma(ref, ref, fs_s.at[1, src], fr.at[1, src], {"tp": over}).wait_recv()
        c = rdma(ref, ref, fs_s.at[2, src], fr.at[2, src], {"tp": mate})
        c.start()
        sends.append(c)
    for k in ks[1:]:
        z_take(1, k)
    for k in ks:
        src = frm(k)
        for lane, who in ((0, mate), (2, (1 - y) * 2 + 1 - core)):
            ref = tok.at[who, src]
            rdma(ref, ref, fs_s.at[lane, src], fr.at[lane, src], {"tp": mate}).wait_recv()
    for m in range(2):
        for k in [0] + ks:
            x_take(m, k)

    tile = 256
    tiles = width // tile

    def hidden(lo, hi):
        @pl.loop(lo * tiles, hi * tiles)
        def _(i):
            b = i // tiles
            cols = pl.ds(pl.multiple_of((i % tiles) * tile, tile), tile)
            gate = jnp.zeros((rows, tile), jnp.float32)
            upper = jnp.zeros((rows, tile), jnp.float32)
            for q in range(nt):
                a = tok[q, b]
                gate += jnp.dot(a, gout[q * quarter:(q + 1) * quarter, cols], preferred_element_type=jnp.float32)
                upper += jnp.dot(a, uout[q * quarter:(q + 1) * quarter, cols], preferred_element_type=jnp.float32)
            hid[b, :, cols] = (gate / (1.0 + jnp.exp(-gate)) * upper).astype(jnp.bfloat16)

    cuts = [nz * (i + 1) // nz for i in range(nz)]
    late = list(ks)
    done = 0
    for i, hi in enumerate(cuts):
        hidden(done, hi)
        done = hi
        if i >= 1 and late:
            z_take(2, late.pop(0))

    def ids(c):
        owner = c // per_owner
        return owner, lax.rem(owner, 2), lax.div(owner, 2), lax.rem(c, per_owner)

    own_down.wait()
    finals = guarded

    def stage_a(i, c):
        mine = pl.ds(pl.multiple_of(c * chunk, chunk), chunk)

        @pl.loop(0, nz)
        def _(b):
            part[c, b] = lax.dot_general(
                hid[b], dout[mine, :], (((1,), (1,)), ((), ())), preferred_element_type=jnp.float32
            ).astype(jnp.bfloat16)

        owner, par, yo, cc = ids(c)
        give = rdma(part.at[c], crx.at[yo * per_owner + cc], cs.at[i], cr.at[i], {"tp": y * 2 + 1 - core})

        @pl.when(par != core)
        def _():
            give.start()
        finals.append((par != core, give))

    def stage_b(i, c):
        owner, par, yo, cc = ids(c)
        up = rdma(part.at[c], yrx.at[cc], ys.at[i], yr.at[i], {"tp": yo * 2 + core})
        away = jnp.logical_and(par == core, yo != y)

        @pl.when(par == core)
        def _():
            slot = crx.at[yo * per_owner + cc]
            rdma(slot, slot, cs.at[i], cr.at[i], {"tp": y * 2 + 1 - core}).wait_recv()

            @pl.loop(0, nz)
            def _(b):
                part[c, b] = (
                    part[c, b].astype(jnp.float32) + crx[yo * per_owner + cc, b].astype(jnp.float32)
                ).astype(jnp.bfloat16)

        @pl.when(away)
        def _():
            up.start()
        finals.append((away, up))

    def stage_c(i, c):
        owner, par, yo, cc = ids(c)
        home = [
            rdma(part.at[c, to(k)], ret.at[z, cc], rs.at[k, cc], rr.at[k, cc], {"fs": to(k)}) for k in ks
        ]

        @pl.when(owner == t)
        def _():
            slot = yrx.at[cc]
            rdma(slot, slot, ys.at[i], yr.at[i], {"tp": (1 - y) * 2 + core}).wait_recv()

            @pl.loop(0, nz)
            def _(b):
                part[c, b] = (
                    part[c, b].astype(jnp.float32) + yrx[cc, b].astype(jnp.float32)
                ).astype(jnp.bfloat16)
            for h in home:
                h.start()
            ret[z, cc] = part[c, z]
        for h in home:
            finals.append((owner == t, h))

    order = [(side, k) for k in [0] + ks for side in (0, 1)]
    lag = 4
    seq = [((g if side == 0 else 1 - g) * nz + frm(k), side, k) for side, k in order]
    n = len(seq)
    for i in range(n + lag):
        if i < n:
            c, side, k = seq[i]
            if side == 1:
                x_take(2, k)
            stage_a(i, c)
        if 0 <= i - 1 < n:
            stage_b(i - 1, seq[i - 1][0])
        if 0 <= i - lag < n:
            stage_c(i - lag, seq[i - lag][0])

    for k in ks:
        for cc in range(per_owner):
            ref = ret.at[frm(k), cc]
            rdma(ref, ref, rs.at[k, cc], rr.at[k, cc], {"fs": to(k)}).wait_recv()
    for cc in range(per_owner):
        total = wt[:, 0:1] * ret[0, cc].astype(jnp.float32)
        for e in range(1, nz):
            total += wt[:, e:e + 1] * ret[e, cc].astype(jnp.float32)
        mixed[:, cc * chunk:(cc + 1) * chunk] = total.astype(jnp.bfloat16)
    for c in sends:
        c.wait_send()
    for flag, c in finals:
        @pl.when(flag)
        def _(c=c):
            c.wait_send()


def fused(ng, nz, nt, tokens, routes, route_weight, gain, w_gate, w_up, w_down):
    scaling = gain[None, :, None]
    gate_local = (w_gate * scaling).astype(jnp.bfloat16)
    up_local = (w_up * scaling).astype(jnp.bfloat16)
    rows, d = tokens.shape
    quarter = d // nt
    experts, chunk, width = w_gate.shape
    chunks = ng * nz
    per_owner = chunks // nt
    ids = jnp.arange(experts, dtype=jnp.int32)
    wt = jnp.sum(jnp.where(routes[:, :, None] == ids, route_weight[:, :, None], 0.0), axis=1)
    bf = jnp.bfloat16
    dma = pltpu.SemaphoreType.DMA
    full = jax.ShapeDtypeStruct((d, width), bf)
    vmem = pl.BlockSpec(memory_space=pltpu.VMEM)
    outs = pl.pallas_call(
        functools.partial(kernel, ng, nz, nt),
        out_shape=(full, full, full, jax.ShapeDtypeStruct((rows, quarter), bf)),
        in_specs=[vmem] * 4 + [pl.BlockSpec(memory_space=pl.ANY)],
        out_specs=(vmem,) * 4,
        scratch_shapes=[
            pltpu.VMEM((nt, nz, rows, quarter), bf),
            pltpu.VMEM((nz, rows, width), bf),
            pltpu.VMEM((chunks, nz, rows, chunk), bf),
            pltpu.VMEM((chunks // 2, nz, rows, chunk), bf),
            pltpu.VMEM((per_owner, nz, rows, chunk), bf),
            pltpu.VMEM((nz, per_owner, rows, chunk), bf),
            dma((2, nz)), dma((nz,)),
            dma((3, nz)), dma((3, nz)), dma,
            dma((3, nz)), dma((3, nz)),
            dma((3, nz)), dma((3, nz)),
            dma((chunks,)), dma((chunks,)),
            dma((chunks,)), dma((chunks,)),
            dma((nz, per_owner)), dma((nz, per_owner)),
        ],
        compiler_params=pltpu.CompilerParams(
            collective_id=0, has_side_effects=True, vmem_limit_bytes=VMEM_LIMIT
        ),
    )(tokens, wt, gate_local, up_local, w_down)
    gate_out, up_out, down_out, mixed = outs
    return (gate_out[None], up_out[None], down_out[None], mixed)

EXP_DEV = 1


def body(tokens, routes, route_weight, gain, w_gate, w_up, w_down):
    scaling = gain[None, :, None]
    gate_local = (w_gate * scaling).astype(jnp.bfloat16)
    up_local = (w_up * scaling).astype(jnp.bfloat16)
    gate_mine, up_mine, down_mine = (
        lax.all_to_all(gate_local, "fs", split_axis=0, concat_axis=1, tiled=True),
        lax.all_to_all(up_local, "fs", split_axis=0, concat_axis=1, tiled=True),
        lax.all_to_all(w_down, "fs", split_axis=0, concat_axis=1, tiled=True),
    )
    gate_out, up_out, down_out = (
        lax.all_gather(gate_mine, "gr", axis=1, tiled=True),
        lax.all_gather(up_mine, "gr", axis=1, tiled=True),
        lax.all_gather(down_mine, "gr", axis=1, tiled=True),
    )
    fs_count = lax.axis_size("fs")
    experts = EXP_DEV * fs_count
    tok_rows = tokens.shape[0]
    capacity = 3 * tok_rows // experts
    float_rows = tokens.astype(jnp.float32)
    normed = (
        float_rows * lax.rsqrt(jnp.mean(float_rows * float_rows, axis=-1, keepdims=True) + EPSILON)
    ).astype(jnp.bfloat16)
    flat_ids = routes.reshape(-1)
    onehot = (flat_ids[:, None] == jnp.arange(experts, dtype=jnp.int32)[None, :]).astype(jnp.int32)
    slot_rank = jnp.sum((jnp.cumsum(onehot, axis=0) - onehot) * onehot, axis=-1)
    destination = (flat_ids * capacity + slot_rank).reshape(tok_rows, 2)
    slot_ids = jnp.arange(experts * capacity, dtype=jnp.int32)
    hits = slot_ids[:, None, None] == destination[None, :, :]
    dispatch = jnp.any(hits, axis=-1).astype(jnp.bfloat16)
    outgoing = jnp.dot(dispatch, normed, preferred_element_type=jnp.float32).astype(jnp.bfloat16)
    outgoing = outgoing.reshape(fs_count, EXP_DEV, capacity, tokens.shape[1])
    arrived = lax.all_to_all(outgoing, "fs", split_axis=0, concat_axis=0, tiled=True)
    gate = jnp.einsum("sjnd,jdf->sjnf", arrived, gate_out, preferred_element_type=jnp.float32)
    upper = jnp.einsum("sjnd,jdf->sjnf", arrived, up_out, preferred_element_type=jnp.float32)
    hidden = (jax.nn.silu(gate) * upper).astype(jnp.bfloat16)
    partial_value = jnp.einsum(
        "sjnf,jdf->sjnd", hidden, down_out, preferred_element_type=jnp.float32
    )
    rounded = lax.optimization_barrier(partial_value.astype(jnp.bfloat16))
    summed = lax.psum_scatter(
        rounded.astype(jnp.float32).astype(jnp.bfloat16), "tp", scatter_dimension=3, tiled=True
    )
    back_home = lax.all_to_all(summed, "fs", split_axis=0, concat_axis=0, tiled=True)
    features = back_home.shape[-1]
    flat_back = back_home.reshape(experts * capacity, features).astype(jnp.float32)
    first = jnp.where(slot_ids[None, :] == destination[:, 0:1], route_weight[:, 0:1], 0.0)
    second = jnp.where(slot_ids[None, :] == destination[:, 1:2], route_weight[:, 1:2], 0.0)
    combine_map = first + second
    mixed = jnp.dot(
        combine_map, flat_back, precision=lax.Precision.HIGHEST, preferred_element_type=jnp.float32
    ).astype(jnp.bfloat16)
    return (gate_out, up_out, down_out, mixed)


def solution(mesh):
    in_specs = (
        P(("gr", "fs"), None),
        P(("gr", "fs"), None),
        P(("gr", "fs"), None),
        P(("gr", "fs")),
        P(None, ("gr", "fs"), "tp"),
        P(None, ("gr", "fs"), "tp"),
        P(None, ("gr", "fs"), "tp"),
    )
    out_specs = (
        P("fs", None, "tp"),
        P("fs", None, "tp"),
        P("fs", None, "tp"),
        P(("gr", "fs"), "tp"),
    )
    ng, nz, nt = mesh.shape["gr"], mesh.shape["fs"], mesh.shape["tp"]
    small = ng == 2 and nt == 4 and nz <= 4
    work = functools.partial(fused, ng, nz, nt) if small else body
    return jax.shard_map(work, mesh=mesh, in_specs=in_specs, out_specs=out_specs, check_vma=False)
```

profile of v0, /device:TPU:12, one launch (start us, length us, event | category | flops | bytes accessed | tf_op | source)
XLA Modules:
  0.0 294.4 jit_solution(8320763540453356149)
XLA Ops:
  0.6 0.7 select_reduce_fusion
  1.4 0.9 copy.13.wt
  2.2 5.9 %multiply_convert_fusion = (bf16[4,256,1024]{2,1,0:T(8,128)(2,1)}, bf16[4,256,1024]{2,1,0:T(8,128)(2,1)}) fusion(bf16[4,256,1024]{2,1,0:T(8,128)(2,1)} %param.12, f32[256]{0:T(256)} %param.10, bf16[4,256,1024]{2,1,0:T(8,128)(2,1)} %param.11), kind=kLoop, calls=%fused_computation | loop fusion | flops 6291456 | bytes 8389632 | tf_op jit(solution)/shard_map/convert_element_type | solution.py:276
  8.2 274.9 %shard_map.102 = (bf16[2048,1024]{1,0:T(8,128)(2,1)}, bf16[2048,1024]{1,0:T(8,128)(2,1)}, bf16[2048,1024]{1,0:T(8,128)(2,1)}, bf16[512,512]{1,0:T(8,128)(2,1)}) custom-call(bf16[512,2048]{1,0:T(8,128)(2,1)} %tok_in.1, f32[512,4]{1,0:T(8,128)} %copy.13.wt, bf16[4,256,1024]{2,1,0:T(8,128)(2,1)} %get-tuple-element.13.gw, ...), custom_call_target="tpu_custom_call" | custom-call | tf_op jit(solution)/shard_map/pallas_call | solution.py:288
  283.0 0.0 copy-start.1
  283.1 4.8 %copy.18 = bf16[1,2048,1024]{2,1,0:T(8,128)(2,1)} copy(bf16[1,2048,1024]{2,1,0:T(8,128)(2,1)} %bitcast.5) | data formatting | bytes 8388608
  287.9 0.0 copy-done.1
  287.9 0.0 copy-start
  287.9 2.1 copy.19
  290.0 1.6 copy-done
  291.6 0.0 copy-start.2
  291.6 2.0 copy.20
  293.6 0.0 copy-done.2
  293.6 0.8 copy.21
Async XLA Ops:
  283.0 4.8 %copy-start.1 = (bf16[2048,1024]{1,0:T(8,128)(2,1)S(1)}, bf16[2048,1024]{1,0:T(8,128)(2,1)}, u32[]{:S(2)}) copy-start(bf16[2048,1024]{1,0:T(8,128)(2,1)} %get-tuple-element.9) | copy-start | bytes 12582916
  287.9 3.7 %copy-start = (bf16[2048,1024]{1,0:T(8,128)(2,1)S(1)}, bf16[2048,1024]{1,0:T(8,128)(2,1)}, u32[]{:S(2)}) copy-start(bf16[2048,1024]{1,0:T(8,128)(2,1)} %get-tuple-element.10) | copy-start | bytes 12582916
  291.6 2.0 copy-start.2
where the time goes:
time: 295 us; the launch traced here: 294 us
  Pallas kernels  275 us (93%)
  local copies, waits for them, and re-layouts  12.2 us (4%)
  other arithmetic  6.66 us (2%)
    pallas_call x1, Pallas kernels, fused(): pl.pallas_call(functools.partial(kernel, ng, nz, nt), out_shape=(full, fu...  275 us
    unnamed x10, local copies, waits for them, and re-layouts  11.3 us
    convert_element_type x1, other arithmetic, fused(): up_local = (w_up * scaling).astype(jnp.bfloat16)  5.94 us

commit v1 on v0

v1 whole, which is shorter than its diff:
```python
import functools
import jax
import jax.numpy as jnp
from jax import lax
from jax.experimental import pallas as pl
from jax.experimental.pallas import tpu as pltpu
from jax.sharding import PartitionSpec as P

MESH = pl.DeviceIdType.MESH
VMEM_LIMIT = 50 * 1024 * 1024
EPSILON = 1e-05
BLOCKS = 4
LAG = 4


def kernel(ng, nz, nt, tok_in, routes, rweight, gain, gw, uw, dw, gout, uout, dout, mixed,
           tok, hid, part, crx, yrx, stage, raw, ret, rly, wsend, wrecv, wcol, gcol,
           ld, ts, tr, fs_s, fr, gs, gr, zs, zr, xs, xr, cs, cr, ys, yr, hs, hr, rs, rr):
    g, z, t = lax.axis_index("gr"), lax.axis_index("fs"), lax.axis_index("tp")
    core, y = lax.rem(t, 2), lax.div(t, 2)
    rows, d = tok_in.shape
    quarter = d // nt
    chunk, width = gw.shape[1], gw.shape[2]
    half = chunk // 2
    chunks = ng * nz
    per_owner = chunks // nt
    nb = BLOCKS
    blk = width // nb
    outs = (gout, uout)
    mate, over = y * 2 + 1 - core, (1 - y) * 2 + core
    inner = jnp.logical_and(z > 0, z < nz - 1)
    side = lax.div(z, 2)
    pair = z + 1 - 2 * lax.rem(z, 2)
    far = (3 * (1 - side), 2 - side)
    order = (far[0], far[1], pair, z)

    def to(k):
        return lax.rem(z + k, nz)

    def frm(k):
        return lax.rem(z + nz - k, nz)

    def rdma(src, dst, ss, rsem, dev):
        return pltpu.make_async_remote_copy(
            src_ref=src, dst_ref=dst, send_sem=ss, recv_sem=rsem, device_id=dev, device_id_type=MESH
        )

    def row0(group, zsrc):
        return pl.multiple_of((group * nz + zsrc) * chunk, chunk)

    def cols(b):
        return pl.ds(pl.multiple_of(b * blk, blk), blk)

    def qcols(q):
        return pl.ds(pl.multiple_of(q * quarter, quarter), quarter)

    def piece(m, b, group, zsrc):
        return outs[m].at[pl.ds(row0(group, zsrc), chunk), cols(b)]

    def dpiece(m, group, zsrc):
        return dout.at[pl.ds(pl.multiple_of(row0(group, zsrc) + m * half, half), half), :]

    def z_copy(m, b, k):
        return rdma(stage.at[m, to(k), :, cols(b)], piece(m, b, g, z), zs.at[m, b, k], zr.at[m, b, k], {"fs": to(k)})

    def zd_copy(m, k):
        return rdma(dw.at[to(k), pl.ds(m * half, half), :], dpiece(m, g, z), zs.at[m, nb, k], zr.at[m, nb, k], {"fs": to(k)})

    def x_own(m, b):
        return rdma(stage.at[m, z, :, cols(b)], piece(m, b, g, z), xs.at[m, b, 0], xr.at[m, b, 0], {"gr": 1 - g})

    def xd_own(m):
        return rdma(dw.at[z, pl.ds(m * half, half), :], dpiece(m, g, z), xs.at[m, nb, 0], xr.at[m, nb, 0], {"gr": 1 - g})

    def relay(ref, m, b, k):
        return rdma(ref, ref, xs.at[m, b, k], xr.at[m, b, k], {"gr": 1 - g})

    def z_arrive(ref, m, b, k):
        rdma(ref, ref, zs.at[m, b, k], zr.at[m, b, k], {"fs": to(k)}).wait_recv()

    def z_take(b, k):
        for m in range(2):
            ref = piece(m, b, g, frm(k))
            z_arrive(ref, m, b, k)
            relay(ref, m, b, k).start()

    def zd_take(k):
        for m in range(2):
            ref = dpiece(m, g, frm(k))
            z_arrive(ref, m, nb, k)
            relay(ref, m, nb, k).start()

    def z_block(b):
        for k in range(1, nz):
            for m in range(2):
                z_copy(m, b, k).start()

    def z_down():
        for k in range(1, nz):
            for m in range(2):
                zd_copy(m, k).start()

    load_tok = pltpu.make_async_copy(tok_in, raw, ld.at[0])
    loads = [pltpu.make_async_copy(src, stage.at[m], ld.at[1 + m]) for m, src in enumerate((gw, uw))]
    own_rows = pl.ds(row0(g, z), chunk)
    own_down = pltpu.make_async_copy(dw.at[z], dout.at[own_rows, :], ld.at[3])
    load_tok.start()
    for c in loads:
        c.start()
    own_down.start()

    barrier = pltpu.get_barrier_semaphore()
    for k in range(1, nz):
        pl.semaphore_signal(barrier, inc=1, device_id={"fs": to(k)}, device_id_type=MESH)
    for who in (mate, over):
        pl.semaphore_signal(barrier, inc=1, device_id={"tp": who}, device_id_type=MESH)
    pl.semaphore_signal(barrier, inc=1, device_id={"gr": 1 - g}, device_id_type=MESH)

    step = 64
    load_tok.wait()

    @pl.loop(0, rows // step)
    def _(i):
        at = pl.ds(pl.multiple_of(i * step, step), step)
        v = raw[at, :].astype(jnp.float32)
        scale = lax.rsqrt(jnp.mean(v * v, axis=-1, keepdims=True) + EPSILON)
        tok[z, at, :] = (v * scale).astype(jnp.bfloat16)

    pl.semaphore_wait(barrier, nz - 1 + 3)

    guarded = []

    def guard(flag, c):
        @pl.when(flag)
        def _():
            c.start()
        guarded.append((flag, c))

    def hop(way, h, src):
        ref = tok.at[src, :, qcols(t)]
        nxt = lax.rem(z + way + nz, nz)
        return rdma(ref, ref, ts.at[(way + 1) // 2, h], tr.at[src], {"fs": nxt})

    right, left = z + 1 < nz, z >= 1
    guard(right, hop(1, 0, z))
    guard(left, hop(-1, 0, z))
    for m in range(2):
        xd_own(m).start()

    gcol[...] = jnp.transpose(jnp.broadcast_to(gain[...], (128, chunk)))
    for c in loads:
        c.wait()

    @pl.loop(0, nz * (chunk // step))
    def _(i):
        e = i // (chunk // step)
        at = pl.ds(pl.multiple_of(lax.rem(i, chunk // step) * step, step), step)
        factor = jnp.concatenate([gcol[at, :]] * (width // 128), axis=1)
        for m in range(2):
            stage[m, e, at, :] = (stage[m, e, at, :].astype(jnp.float32) * factor).astype(jnp.bfloat16)

    z_block(0)

    @pl.when(jnp.logical_not(inner))
    def _():
        @pl.loop(1, nb)
        def _(b):
            z_block(b)
        z_down()

    for b in range(min(2, nb)):
        for m in range(2):
            x_own(m, b).start()

    for e in range(nz):
        wsend[e] = (
            jnp.where(routes[0:1, :] == e, rweight[0:1, :], 0.0)
            + jnp.where(routes[1:2, :] == e, rweight[1:2, :], 0.0)
        )
    wrecv[z] = wsend[z]
    for k in range(1, nz):
        rdma(wsend.at[to(k)], wrecv.at[z], gs.at[k], gr.at[k], {"fs": to(k)}).start()
    for m in range(2):
        outs[m][own_rows, :] = stage[m, z]

    for h in range(1, nz):
        for way in (1, -1):
            src = lax.rem(z - way * h + nz, nz)
            valid = z >= h if way == 1 else z + h < nz
            more = right if way == 1 else left
            ref = tok.at[src, :, qcols(t)]

            @pl.when(valid)
            def _(ref=ref, src=src):
                rdma(ref, ref, ts.at[0, 0], tr.at[src], {"fs": lax.rem(z + 1, nz)}).wait_recv()
            guard(jnp.logical_and(valid, more), hop(way, h, src))
            guard(valid, rdma(ref, ref, fs_s.at[1, src], fr.at[1, src], {"tp": over}))
            guard(valid, rdma(ref, ref, fs_s.at[0, src], fr.at[0, src], {"tp": mate}))
        if h == 1:
            @pl.when(inner)
            def _():
                z_block(1)
            z_take(0, 1)
        if h == 2:
            @pl.when(inner)
            def _():
                @pl.loop(2, nb)
                def _(b):
                    z_block(b)
            for k in range(2, nz):
                z_take(0, k)
            for b in range(2, nb):
                for m in range(2):
                    x_own(m, b).start()

    def token_quarter(lane, src, q):
        ref = tok.at[src, :, qcols(q)]
        return rdma(ref, ref, fs_s.at[lane, src], fr.at[lane, src], {"tp": mate})

    @pl.loop(nz, (nb + 1) * nz)
    def _(i):
        b, s = i // nz, lax.rem(i, nz)
        src = frm(s)
        k = s + 1
        take = s < nz - 1

        @pl.when(jnp.logical_and(take, b < nb))
        def _():
            z_take(b, k)

        @pl.when(jnp.logical_and(take, b == nb))
        def _():
            zd_take(k)

        @pl.when(jnp.logical_and(inner, i == nb * nz - 2))
        def _():
            z_down()

        @pl.when(s == 0)
        def _():
            @pl.loop(0, nz)
            def _(kk):
                for m in range(2):
                    ref = piece(m, b - 1, 1 - g, frm(kk))
                    rdma(ref, ref, xs.at[m, b - 1, kk], xr.at[m, b - 1, kk], {"gr": 1 - g}).wait_recv()

        @pl.when(b == 1)
        def _():
            @pl.when(s >= 1)
            def _():
                token_quarter(1, src, over).wait_recv()
                token_quarter(2, src, over).start()
                token_quarter(0, src, mate).wait_recv()
                token_quarter(2, src, (1 - y) * 2 + 1 - core).wait_recv()
                rdma(wrecv.at[src], wrecv.at[src], gs.at[s], gr.at[s], {"fs": to(s)}).wait_recv()
            wcol[src] = jnp.transpose(jnp.broadcast_to(wrecv[src], (128, rows)))

        a = tok[src]
        gate = jnp.dot(a, gout[:, cols(b - 1)], preferred_element_type=jnp.float32)
        upper = jnp.dot(a, uout[:, cols(b - 1)], preferred_element_type=jnp.float32)
        weight = jnp.concatenate([wcol[src]] * (blk // 128), axis=1)
        hid[src, :, cols(b - 1)] = (gate / (1.0 + jnp.exp(-gate)) * upper * weight).astype(jnp.bfloat16)

    own_down.wait()

    def chunk_of(i):
        k, other = i // 2, lax.rem(i, 2)
        group = g + other * (1 - 2 * g)
        c = group * nz + frm(k)
        owner = c // per_owner
        return k, other, c, owner, lax.rem(owner, 2), owner // 2, lax.rem(c, per_owner)

    def give(i):
        k, other, c, owner, par, yo, cc = chunk_of(i)
        return rdma(part.at[c], crx.at[yo * per_owner + cc], cs.at[i], cr.at[i], {"tp": mate})

    def up(i, j):
        k, other, c, owner, par, yo, cc = chunk_of(i)
        return rdma(part.at[c, order[j]], yrx.at[cc, order[j]], ys.at[i, j], yr.at[i, j], {"tp": over})

    def near(c, cc, j):
        dst = rly.at[j, cc] if j < 2 else ret.at[0, cc]
        return rdma(part.at[c, order[j]], dst, hs.at[j, cc], hr.at[j, cc], {"fs": pair})

    def cross(cc, j):
        return rdma(part.at[t * per_owner + cc, order[j]], ret.at[1, cc], rs.at[j, cc], rr.at[cc], {"fs": order[j]})

    def stage_a(i):
        k, other, c, owner, par, yo, cc = chunk_of(i)

        @pl.when(other == 1)
        def _():
            for m in range(2):
                ref = dpiece(m, 1 - g, frm(k))
                rdma(ref, ref, xs.at[m, nb, k], xr.at[m, nb, k], {"gr": 1 - g}).wait_recv()

        mine = pl.ds(pl.multiple_of(c * chunk, chunk), chunk)

        @pl.loop(0, nz)
        def _(b):
            part[c, b] = lax.dot_general(
                hid[b], dout[mine, :], (((1,), (1,)), ((), ())), preferred_element_type=jnp.float32
            ).astype(jnp.bfloat16)

        @pl.when(par != core)
        def _():
            give(i).start()

    def stage_b(i):
        k, other, c, owner, par, yo, cc = chunk_of(i)

        @pl.when(par == core)
        def _():
            slot = crx.at[yo * per_owner + cc]
            rdma(slot, slot, cs.at[i], cr.at[i], {"tp": mate}).wait_recv()
            for j in range(nz):
                b = order[j]
                part[c, b] = (
                    part[c, b].astype(jnp.float32) + crx[yo * per_owner + cc, b].astype(jnp.float32)
                ).astype(jnp.bfloat16)

                @pl.when(yo != y)
                def _(j=j):
                    up(i, j).start()

    def stage_c(i):
        k, other, c, owner, par, yo, cc = chunk_of(i)

        @pl.when(owner == t)
        def _():
            for j in range(nz):
                b = order[j]
                slot = yrx.at[cc, b]
                rdma(slot, slot, ys.at[i, j], yr.at[i, j], {"tp": over}).wait_recv()
                part[c, b] = (
                    part[c, b].astype(jnp.float32) + yrx[cc, b].astype(jnp.float32)
                ).astype(jnp.bfloat16)
                if j < 2:
                    @pl.when(jnp.logical_not(inner))
                    def _(j=j):
                        near(c, cc, j).start()
                elif j == 2:
                    near(c, cc, j).start()

    n = chunks

    @pl.loop(0, n + LAG)
    def _(i):
        @pl.when(i < n)
        def _():
            stage_a(i)

        @pl.when(jnp.logical_and(i >= 1, i - 1 < n))
        def _():
            stage_b(i - 1)

        @pl.when(i >= LAG)
        def _():
            stage_c(i - LAG)

    @pl.when(inner)
    def _():
        first = jnp.where(side == core, 0, 1)
        for turn in range(per_owner):
            cc = first + turn * (1 - 2 * first)
            for j in range(2):
                slot = rly.at[j, cc]
                rdma(slot, slot, hs.at[j, cc], hr.at[j, cc], {"fs": pair}).wait_recv()
                c, b = t * per_owner + cc, order[j]
                part[c, b] = (
                    part[c, b].astype(jnp.float32) + rly[j, cc].astype(jnp.float32)
                ).astype(jnp.bfloat16)
                cross(cc, j).start()

    for cc in range(per_owner):
        direct, crossed = ret.at[0, cc], ret.at[1, cc]
        rdma(direct, direct, hs.at[2, cc], hr.at[2, cc], {"fs": pair}).wait_recv()
        rdma(crossed, crossed, rs.at[0, cc], rr.at[cc], {"fs": pair}).wait_recv()
        mixed[:, cc * chunk:(cc + 1) * chunk] = (
            part[t * per_owner + cc, z].astype(jnp.float32)
            + ret[0, cc].astype(jnp.float32)
            + ret[1, cc].astype(jnp.float32)
        ).astype(jnp.bfloat16)

    @pl.loop(1, nz)
    def _(k):
        rdma(wsend.at[to(k)], wrecv.at[z], gs.at[k], gr.at[k], {"fs": to(k)}).wait_send()
        for m in range(2):
            zd_copy(m, k).wait_send()
            relay(dpiece(m, g, frm(k)), m, nb, k).wait_send()
        token_quarter(2, frm(k), over).wait_send()

        @pl.loop(0, nb)
        def _(b):
            for m in range(2):
                z_copy(m, b, k).wait_send()
                relay(piece(m, b, g, frm(k)), m, b, k).wait_send()

    for m in range(2):
        xd_own(m).wait_send()

        @pl.loop(0, nb)
        def _(b):
            x_own(m, b).wait_send()

    for flag, c in guarded:
        @pl.when(flag)
        def _(c=c):
            c.wait_send()

    @pl.loop(0, n)
    def _(i):
        k, other, c, owner, par, yo, cc = chunk_of(i)

        @pl.when(par != core)
        def _():
            give(i).wait_send()

        @pl.when(jnp.logical_and(par == core, yo != y))
        def _():
            for j in range(nz):
                up(i, j).wait_send()

    for cc in range(per_owner):
        c = t * per_owner + cc
        near(c, cc, 2).wait_send()
        for j in range(2):
            @pl.when(inner)
            def _(j=j, cc=cc):
                cross(cc, j).wait_send()

            @pl.when(jnp.logical_not(inner))
            def _(j=j, c=c, cc=cc):
                near(c, cc, j).wait_send()


def store(gate, upper, down, mixed, gate_out, up_out, down_out, mixed_out, sem):
    copies = [
        pltpu.make_async_copy(gate, gate_out.at[0], sem.at[0]),
        pltpu.make_async_copy(upper, up_out.at[0], sem.at[1]),
        pltpu.make_async_copy(down, down_out.at[0], sem.at[2]),
        pltpu.make_async_copy(mixed, mixed_out, sem.at[3]),
    ]
    for c in copies:
        c.start()
    for c in copies:
        c.wait()


def fused(ng, nz, nt, tokens, routes, route_weight, gain, w_gate, w_up, w_down):
    rows, d = tokens.shape
    quarter = d // nt
    experts, chunk, width = w_gate.shape
    chunks = ng * nz
    per_owner = chunks // nt
    bf, f32 = jnp.bfloat16, jnp.float32
    dma = pltpu.SemaphoreType.DMA
    full = pltpu.VMEM((d, width), bf)
    vmem = pl.BlockSpec(memory_space=pltpu.VMEM)
    anywhere = pl.BlockSpec(memory_space=pl.ANY)
    results = pl.pallas_call(
        functools.partial(kernel, ng, nz, nt),
        out_shape=(full, full, full, pltpu.VMEM((rows, quarter), bf)),
        in_specs=[anywhere, vmem, vmem, vmem, anywhere, anywhere, anywhere],
        out_specs=(vmem,) * 4,
        scratch_shapes=[
            pltpu.VMEM((nz, rows, d), bf),
            pltpu.VMEM((nz, rows, width), bf),
            pltpu.VMEM((chunks, nz, rows, chunk), bf),
            pltpu.VMEM((chunks // 2, nz, rows, chunk), bf),
            pltpu.VMEM((per_owner, nz, rows, chunk), bf),
            pltpu.VMEM((2, nz, chunk, width), bf),
            pltpu.VMEM((rows, d), bf),
            pltpu.VMEM((2, per_owner, rows, chunk), bf),
            pltpu.VMEM((2, per_owner, rows, chunk), bf),
            pltpu.VMEM((nz, 1, rows), f32),
            pltpu.VMEM((nz, 1, rows), f32),
            pltpu.VMEM((nz, rows, 128), f32),
            pltpu.VMEM((chunk, 128), f32),
            dma((4,)),
            dma((2, nz)), dma((nz,)),
            dma((3, nz)), dma((3, nz)),
            dma((nz,)), dma((nz,)),
            dma((2, BLOCKS + 1, nz)), dma((2, BLOCKS + 1, nz)),
            dma((2, BLOCKS + 1, nz)), dma((2, BLOCKS + 1, nz)),
            dma((chunks,)), dma((chunks,)),
            dma((chunks, nz)), dma((chunks, nz)),
            dma((3, per_owner)), dma((3, per_owner)),
            dma((2, per_owner)), dma((per_owner,)),
        ],
        compiler_params=pltpu.CompilerParams(
            collective_id=0, has_side_effects=True, vmem_limit_bytes=VMEM_LIMIT
        ),
    )(tokens, routes.T, route_weight.T, gain.reshape(1, chunk), w_gate, w_up, w_down)
    whole = jax.ShapeDtypeStruct((1, d, width), bf)
    return pl.pallas_call(
        store,
        out_shape=(whole, whole, whole, jax.ShapeDtypeStruct((rows, quarter), bf)),
        in_specs=[vmem] * 4,
        out_specs=(anywhere,) * 4,
        scratch_shapes=[dma((4,))],
        compiler_params=pltpu.CompilerParams(vmem_limit_bytes=4 * 1024 * 1024),
    )(*results)

EXP_DEV = 1


def body(tokens, routes, route_weight, gain, w_gate, w_up, w_down):
    scaling = gain[None, :, None]
    gate_local = (w_gate * scaling).astype(jnp.bfloat16)
    up_local = (w_up * scaling).astype(jnp.bfloat16)
    gate_mine, up_mine, down_mine = (
        lax.all_to_all(gate_local, "fs", split_axis=0, concat_axis=1, tiled=True),
        lax.all_to_all(up_local, "fs", split_axis=0, concat_axis=1, tiled=True),
        lax.all_to_all(w_down, "fs", split_axis=0, concat_axis=1, tiled=True),
    )
    gate_out, up_out, down_out = (
        lax.all_gather(gate_mine, "gr", axis=1, tiled=True),
        lax.all_gather(up_mine, "gr", axis=1, tiled=True),
        lax.all_gather(down_mine, "gr", axis=1, tiled=True),
    )
    fs_count = lax.axis_size("fs")
    experts = EXP_DEV * fs_count
    tok_rows = tokens.shape[0]
    capacity = 3 * tok_rows // experts
    float_rows = tokens.astype(jnp.float32)
    normed = (
        float_rows * lax.rsqrt(jnp.mean(float_rows * float_rows, axis=-1, keepdims=True) + EPSILON)
    ).astype(jnp.bfloat16)
    flat_ids = routes.reshape(-1)
    onehot = (flat_ids[:, None] == jnp.arange(experts, dtype=jnp.int32)[None, :]).astype(jnp.int32)
    slot_rank = jnp.sum((jnp.cumsum(onehot, axis=0) - onehot) * onehot, axis=-1)
    destination = (flat_ids * capacity + slot_rank).reshape(tok_rows, 2)
    slot_ids = jnp.arange(experts * capacity, dtype=jnp.int32)
    hits = slot_ids[:, None, None] == destination[None, :, :]
    dispatch = jnp.any(hits, axis=-1).astype(jnp.bfloat16)
    outgoing = jnp.dot(dispatch, normed, preferred_element_type=jnp.float32).astype(jnp.bfloat16)
    outgoing = outgoing.reshape(fs_count, EXP_DEV, capacity, tokens.shape[1])
    arrived = lax.all_to_all(outgoing, "fs", split_axis=0, concat_axis=0, tiled=True)
    gate = jnp.einsum("sjnd,jdf->sjnf", arrived, gate_out, preferred_element_type=jnp.float32)
    upper = jnp.einsum("sjnd,jdf->sjnf", arrived, up_out, preferred_element_type=jnp.float32)
    hidden = (jax.nn.silu(gate) * upper).astype(jnp.bfloat16)
    partial_value = jnp.einsum(
        "sjnf,jdf->sjnd", hidden, down_out, preferred_element_type=jnp.float32
    )
    rounded = lax.optimization_barrier(partial_value.astype(jnp.bfloat16))
    summed = lax.psum_scatter(
        rounded.astype(jnp.float32).astype(jnp.bfloat16), "tp", scatter_dimension=3, tiled=True
    )
    back_home = lax.all_to_all(summed, "fs", split_axis=0, concat_axis=0, tiled=True)
    features = back_home.shape[-1]
    flat_back = back_home.reshape(experts * capacity, features).astype(jnp.float32)
    first = jnp.where(slot_ids[None, :] == destination[:, 0:1], route_weight[:, 0:1], 0.0)
    second = jnp.where(slot_ids[None, :] == destination[:, 1:2], route_weight[:, 1:2], 0.0)
    combine_map = first + second
    mixed = jnp.dot(
        combine_map, flat_back, precision=lax.Precision.HIGHEST, preferred_element_type=jnp.float32
    ).astype(jnp.bfloat16)
    return (gate_out, up_out, down_out, mixed)


def solution(mesh):
    in_specs = (
        P(("gr", "fs"), None),
        P(("gr", "fs"), None),
        P(("gr", "fs"), None),
        P(("gr", "fs")),
        P(None, ("gr", "fs"), "tp"),
        P(None, ("gr", "fs"), "tp"),
        P(None, ("gr", "fs"), "tp"),
    )
    out_specs = (
        P("fs", None, "tp"),
        P("fs", None, "tp"),
        P("fs", None, "tp"),
        P(("gr", "fs"), "tp"),
    )
    ng, nz, nt = mesh.shape["gr"], mesh.shape["fs"], mesh.shape["tp"]
    small = ng == 2 and nt == 4 and nz == 4
    work = functools.partial(fused, ng, nz, nt) if small else body
    return jax.shard_map(work, mesh=mesh, in_specs=in_specs, out_specs=out_specs, check_vma=False)
```

time: 295 us -> 254 us (0.86)
  Pallas kernels: 275 us -> 250 us
  local copies, waits for them, and re-layouts: 12.2 us -> 0 us
  other arithmetic: 6.66 us -> 0 us
    pallas_call x1, Pallas kernels: 275 us -> 245 us  [fused(): pl.pallas_call(functools.partial(kernel, ng, nz, nt), out_shape=(full, fu...]
    unnamed x10 -> x0, local copies, waits for them, and re-layouts: 11.3 us -> none
    convert_element_type x1 -> x0, other arithmetic: 5.94 us -> none  [fused(): up_local = (w_up * scaling).astype(jnp.bfloat16)]
    pallas_call x0 -> x1, Pallas kernels: none -> 4.73 us  [fused(): pl.pallas_call(store, out_shape=(whole, whole, whole, jax.ShapeDtypeStruc...]
where the time goes in v1:
time: 254 us; the launch traced here: 251 us
  Pallas kernels  250 us (98%)
    pallas_call x1, Pallas kernels, fused(): pl.pallas_call(functools.partial(kernel, ng, nz, nt), out_shape=(full, fu...  245 us

profile of v1, /device:TPU:12, one launch (start us, length us, event | category | flops | bytes accessed | tf_op | source)
XLA Modules:
  0.0 250.7 jit_solution(16535801584630517942)
XLA Ops:
  0.6 245.3 %shard_map.102 = (bf16[2048,1024]{1,0:T(8,128)(2,1)S(1)}, bf16[2048,1024]{1,0:T(8,128)(2,1)S(1)}, bf16[2048,1024]{1,0:T(8,128)(2,1)S(1)}, bf16[512,512]{1,0:T(8,128)(2,1)S(1)}) custom-call(bf16[512,2048]{1,0:T(8,128)(2,1)} %tok_in.1, s32[2,512]{1,0:T(2,128)} %bitcast.3, f32[2,512]{1,0:T(2,128)} %bitcast.4, f32[1,256]{1,0:T(1,128)} %bitcast.5, ...), custom_call_target="tpu_custom_call" | custom-call | tf_op jit(solution)/shard_map/pallas_call | solution.py:461
  245.9 4.7 %shard_map.103 = (bf16[1,2048,1024]{2,1,0:T(8,128)(2,1)}, bf16[1,2048,1024]{2,1,0:T(8,128)(2,1)}, bf16[1,2048,1024]{2,1,0:T(8,128)(2,1)}, bf16[512,512]{1,0:T(8,128)(2,1)}) custom-call(bf16[2048,1024]{1,0:T(8,128)(2,1)S(1)} %get-tuple-element.8.gate, bf16[2048,1024]{1,0:T(8,128)(2,1)S(1)} %get-tuple-element.9.upper, ...), custom_call_target="tpu_custom_call" | custom-call | tf_op jit(solution)/shard_map/pallas_call | solution.py:496

commit v2 on v1

--- a/solution.py
+++ b/solution.py
@@ -33,6 +33,11 @@
     pair = z + 1 - 2 * lax.rem(z, 2)
     far = (3 * (1 - side), 2 - side)
     order = (far[0], far[1], pair, z)
+    odd = lax.rem(z, 2)
+    k_near = 3 - 2 * odd
+    near_to = 4 - k_near
+    k_mid = jnp.where(inner, near_to, 2)
+    k_far = jnp.where(inner, 2, near_to)
 
     def to(k):
         return lax.rem(z + k, nz)
@@ -90,13 +95,23 @@
             z_arrive(ref, m, nb, k)
             relay(ref, m, nb, k).start()
 
-    def z_block(b):
-        for k in range(1, nz):
+    def order_of(j):
+        return jnp.where(j == 0, far[0], jnp.where(j == 1, far[1], jnp.where(j == 2, pair, z)))
+
+    def k_of(s):
+        return jnp.where(s == 0, 0, jnp.where(s == 1, k_near, jnp.where(s == 2, k_far, k_mid)))
+
+    def z_cross(b):
+        for k in (2, k_near):
             for m in range(2):
                 z_copy(m, b, k).start()
 
+    def z_side(b):
+        for m in range(2):
+            z_copy(m, b, near_to).start()
+
     def z_down():
-        for k in range(1, nz):
+        for k in (near_to, 2, k_near):
             for m in range(2):
                 zd_copy(m, k).start()
 
@@ -117,15 +132,18 @@
     pl.semaphore_signal(barrier, inc=1, device_id={"gr": 1 - g}, device_id_type=MESH)
 
     step = 64
-    load_tok.wait()
-
-    @pl.loop(0, rows // step)
-    def _(i):
-        at = pl.ds(pl.multiple_of(i * step, step), step)
-        v = raw[at, :].astype(jnp.float32)
-        scale = lax.rsqrt(jnp.mean(v * v, axis=-1, keepdims=True) + EPSILON)
-        tok[z, at, :] = (v * scale).astype(jnp.bfloat16)
-
+
+    def norm():
+        load_tok.wait()
+
+        @pl.loop(0, rows // step)
+        def _(i):
+            at = pl.ds(pl.multiple_of(i * step, step), step)
+            v = raw[at, :].astype(jnp.float32)
+            scale = lax.rsqrt(jnp.mean(v * v, axis=-1, keepdims=True) + EPSILON)
+            tok[z, at, :] = (v * scale).astype(jnp.bfloat16)
+
+    norm()
     pl.semaphore_wait(barrier, nz - 1 + 3)
 
     guarded = []
@@ -147,28 +165,30 @@
     for m in range(2):
         xd_own(m).start()
 
-    gcol[...] = jnp.transpose(jnp.broadcast_to(gain[...], (128, chunk)))
-    for c in loads:
-        c.wait()
-
-    @pl.loop(0, nz * (chunk // step))
-    def _(i):
-        e = i // (chunk // step)
-        at = pl.ds(pl.multiple_of(lax.rem(i, chunk // step) * step, step), step)
-        factor = jnp.concatenate([gcol[at, :]] * (width // 128), axis=1)
-        for m in range(2):
-            stage[m, e, at, :] = (stage[m, e, at, :].astype(jnp.float32) * factor).astype(jnp.bfloat16)
-
-    z_block(0)
-
+    def scaleall():
+        gcol[...] = jnp.transpose(jnp.broadcast_to(gain[...], (128, chunk)))
+        for c in loads:
+            c.wait()
+
+        @pl.loop(0, nz * (chunk // step))
+        def _(i):
+            e = i // (chunk // step)
+            at = pl.ds(pl.multiple_of(lax.rem(i, chunk // step) * step, step), step)
+            factor = jnp.concatenate([gcol[at, :]] * (width // 128), axis=1)
+            for m in range(2):
+                stage[m, e, at, :] = (stage[m, e, at, :].astype(jnp.float32) * factor).astype(jnp.bfloat16)
+
+    scaleall()
     @pl.when(jnp.logical_not(inner))
     def _():
-        @pl.loop(1, nb)
-        def _(b):
-            z_block(b)
-        z_down()
-
-    for b in range(min(2, nb)):
+        pl.loop(0, nb)(z_side)
+        pl.loop(0, nb)(z_cross)
+
+    @pl.when(inner)
+    def _():
+        z_side(0)
+
+    for b in range(nb):
         for m in range(2):
             x_own(m, b).start()
 
@@ -183,7 +203,7 @@
     for m in range(2):
         outs[m][own_rows, :] = stage[m, z]
 
-    for h in range(1, nz):
+    def hops(h):
         for way in (1, -1):
             src = lax.rem(z - way * h + nz, nz)
             valid = z >= h if way == 1 else z + h < nz
@@ -196,83 +216,107 @@
             guard(jnp.logical_and(valid, more), hop(way, h, src))
             guard(valid, rdma(ref, ref, fs_s.at[1, src], fr.at[1, src], {"tp": over}))
             guard(valid, rdma(ref, ref, fs_s.at[0, src], fr.at[0, src], {"tp": mate}))
-        if h == 1:
-            @pl.when(inner)
-            def _():
-                z_block(1)
-            z_take(0, 1)
-        if h == 2:
-            @pl.when(inner)
-            def _():
-                @pl.loop(2, nb)
-                def _(b):
-                    z_block(b)
-            for k in range(2, nz):
-                z_take(0, k)
-            for b in range(2, nb):
-                for m in range(2):
-                    x_own(m, b).start()
+
+    def take_near(lo, hi):
+        @pl.loop(lo, hi)
+        def _(b):
+            z_take(b, k_near)
+
+    hops(1)
+
+    @pl.when(inner)
+    def _():
+        z_cross(0)
+        take_near(0, nb // 2)
+    hops(2)
+
+    @pl.when(inner)
+    def _():
+        pl.loop(1, nb)(z_side)
+        pl.loop(1, nb)(z_cross)
+        z_down()
+        take_near(nb // 2, nb)
+    for h in range(3, nz):
+        hops(h)
+
+    z_take(0, k_mid)
+
+    @pl.loop(0, nb)
+    def _(b):
+        z_take(b, k_far)
+
+        @pl.when(jnp.logical_and(jnp.logical_not(inner), lax.rem(b, 2) == 0))
+        def _():
+            z_take(b // 2, k_near)
 
     def token_quarter(lane, src, q):
         ref = tok.at[src, :, qcols(q)]
         return rdma(ref, ref, fs_s.at[lane, src], fr.at[lane, src], {"tp": mate})
 
+    def x_wait(b):
+        @pl.loop(0, nz)
+        def _(kk):
+            for m in range(2):
+                ref = piece(m, b, 1 - g, frm(kk))
+                rdma(ref, ref, xs.at[m, b, kk], xr.at[m, b, kk], {"gr": 1 - g}).wait_recv()
+
+    def tok_wait(src, s):
+        token_quarter(1, src, over).wait_recv()
+        token_quarter(2, src, over).start()
+        token_quarter(0, src, mate).wait_recv()
+        token_quarter(2, src, (1 - y) * 2 + 1 - core).wait_recv()
+        rdma(wrecv.at[src], wrecv.at[src], gs.at[s], gr.at[s], {"fs": to(s)}).wait_recv()
+
+    def hidden(b, src):
+        a = tok[src]
+        gate = jnp.dot(a, gout[:, cols(b)], preferred_element_type=jnp.float32)
+        upper = jnp.dot(a, uout[:, cols(b)], preferred_element_type=jnp.float32)
+        weight = jnp.concatenate([wcol[src]] * (blk // 128), axis=1)
+        hid[src, :, cols(b)] = (gate / (1.0 + jnp.exp(-gate)) * upper * weight).astype(jnp.bfloat16)
+
     @pl.loop(nz, (nb + 1) * nz)
     def _(i):
         b, s = i // nz, lax.rem(i, nz)
-        src = frm(s)
-        k = s + 1
-        take = s < nz - 1
-
-        @pl.when(jnp.logical_and(take, b < nb))
-        def _():
-            z_take(b, k)
-
-        @pl.when(jnp.logical_and(take, b == nb))
-        def _():
-            zd_take(k)
-
-        @pl.when(jnp.logical_and(inner, i == nb * nz - 2))
+        src = frm(k_of(s))
+
+        @pl.when(jnp.logical_and(s == 0, b < nb))
+        def _():
+            z_take(b, k_mid)
+
+        @pl.when(jnp.logical_and(jnp.logical_not(inner), jnp.logical_and(s == 1, b < (nb + 1) // 2 + 1)))
+        def _():
+            z_take(b + nb // 2 - 1, k_near)
+
+        @pl.when(jnp.logical_and(jnp.logical_not(inner), i == (nb - 1) * nz))
         def _():
             z_down()
 
         @pl.when(s == 0)
         def _():
-            @pl.loop(0, nz)
-            def _(kk):
-                for m in range(2):
-                    ref = piece(m, b - 1, 1 - g, frm(kk))
-                    rdma(ref, ref, xs.at[m, b - 1, kk], xr.at[m, b - 1, kk], {"gr": 1 - g}).wait_recv()
+            x_wait(b - 1)
 
         @pl.when(b == 1)
         def _():
             @pl.when(s >= 1)
             def _():
-                token_quarter(1, src, over).wait_recv()
-                token_quarter(2, src, over).start()
-                token_quarter(0, src, mate).wait_recv()
-                token_quarter(2, src, (1 - y) * 2 + 1 - core).wait_recv()
-                rdma(wrecv.at[src], wrecv.at[src], gs.at[s], gr.at[s], {"fs": to(s)}).wait_recv()
+                tok_wait(src, k_of(s))
             wcol[src] = jnp.transpose(jnp.broadcast_to(wrecv[src], (128, rows)))
 
-        a = tok[src]
-        gate = jnp.dot(a, gout[:, cols(b - 1)], preferred_element_type=jnp.float32)
-        upper = jnp.dot(a, uout[:, cols(b - 1)], preferred_element_type=jnp.float32)
-        weight = jnp.concatenate([wcol[src]] * (blk // 128), axis=1)
-        hid[src, :, cols(b - 1)] = (gate / (1.0 + jnp.exp(-gate)) * upper * weight).astype(jnp.bfloat16)
+        hidden(b - 1, src)
 
     own_down.wait()
 
     def chunk_of(i):
-        k, other = i // 2, lax.rem(i, 2)
+        k, other = k_of(i // 2), lax.rem(i, 2)
         group = g + other * (1 - 2 * g)
         c = group * nz + frm(k)
         owner = c // per_owner
         return k, other, c, owner, lax.rem(owner, 2), owner // 2, lax.rem(c, per_owner)
 
-    def give(i):
+    def give(i, j):
         k, other, c, owner, par, yo, cc = chunk_of(i)
-        return rdma(part.at[c], crx.at[yo * per_owner + cc], cs.at[i], cr.at[i], {"tp": mate})
+        b = order_of(j)
+        return rdma(part.at[c, b], crx.at[yo * per_owner + cc, b], cs.at[i, j], cr.at[i, j], {"tp": mate})
 
     def up(i, j):
         k, other, c, owner, par, yo, cc = chunk_of(i)
@@ -285,36 +329,40 @@
     def cross(cc, j):
         return rdma(part.at[t * per_owner + cc, order[j]], ret.at[1, cc], rs.at[j, cc], rr.at[cc], {"fs": order[j]})
 
+    def x_down_wait(k):
+        for m in range(2):
+            ref = dpiece(m, 1 - g, frm(k))
+            rdma(ref, ref, xs.at[m, nb, k], xr.at[m, nb, k], {"gr": 1 - g}).wait_recv()
+
     def stage_a(i):
         k, other, c, owner, par, yo, cc = chunk_of(i)
 
         @pl.when(other == 1)
         def _():
-            for m in range(2):
-                ref = dpiece(m, 1 - g, frm(k))
-                rdma(ref, ref, xs.at[m, nb, k], xr.at[m, nb, k], {"gr": 1 - g}).wait_recv()
+            x_down_wait(k)
 
         mine = pl.ds(pl.multiple_of(c * chunk, chunk), chunk)
 
         @pl.loop(0, nz)
-        def _(b):
+        def _(j):
+            b = order_of(j)
             part[c, b] = lax.dot_general(
                 hid[b], dout[mine, :], (((1,), (1,)), ((), ())), preferred_element_type=jnp.float32
             ).astype(jnp.bfloat16)
 
-        @pl.when(par != core)
-        def _():
-            give(i).start()
+            @pl.when(par != core)
+            def _():
+                give(i, j).start()
 
     def stage_b(i):
         k, other, c, owner, par, yo, cc = chunk_of(i)
 
         @pl.when(par == core)
         def _():
-            slot = crx.at[yo * per_owner + cc]
-            rdma(slot, slot, cs.at[i], cr.at[i], {"tp": mate}).wait_recv()
             for j in range(nz):
                 b = order[j]
+                slot = crx.at[yo * per_owner + cc, b]
+                rdma(slot, slot, cs.at[i, j], cr.at[i, j], {"tp": mate}).wait_recv()
                 part[c, b] = (
                     part[c, b].astype(jnp.float32) + crx[yo * per_owner + cc, b].astype(jnp.float32)
                 ).astype(jnp.bfloat16)
@@ -346,20 +394,20 @@
 
     @pl.loop(0, n + LAG)
     def _(i):
+        @pl.when(jnp.logical_or(i == 2, jnp.logical_or(i == 3, i == 5)))
+        def _():
+            zd_take(k_of((i + 1) // 2))
+
         @pl.when(i < n)
         def _():
             stage_a(i)
-
-        @pl.when(jnp.logical_and(i >= 1, i - 1 < n))
-        def _():
-            stage_b(i - 1)
+            stage_b(i)
 
         @pl.when(i >= LAG)
         def _():
             stage_c(i - LAG)
 
-    @pl.when(inner)
-    def _():
+    def cross_phase():
         first = jnp.where(side == core, 0, 1)
         for turn in range(per_owner):
             cc = first + turn * (1 - 2 * first)
@@ -372,66 +420,75 @@
                 ).astype(jnp.bfloat16)
                 cross(cc, j).start()
 
-    for cc in range(per_owner):
-        direct, crossed = ret.at[0, cc], ret.at[1, cc]
-        rdma(direct, direct, hs.at[2, cc], hr.at[2, cc], {"fs": pair}).wait_recv()
-        rdma(crossed, crossed, rs.at[0, cc], rr.at[cc], {"fs": pair}).wait_recv()
-        mixed[:, cc * chunk:(cc + 1) * chunk] = (
-            part[t * per_owner + cc, z].astype(jnp.float32)
-            + ret[0, cc].astype(jnp.float32)
-            + ret[1, cc].astype(jnp.float32)
-        ).astype(jnp.bfloat16)
-
-    @pl.loop(1, nz)
-    def _(k):
-        rdma(wsend.at[to(k)], wrecv.at[z], gs.at[k], gr.at[k], {"fs": to(k)}).wait_send()
+    pl.when(inner)(cross_phase)
+
+    def final():
+        for cc in range(per_owner):
+            direct, crossed = ret.at[0, cc], ret.at[1, cc]
+            rdma(direct, direct, hs.at[2, cc], hr.at[2, cc], {"fs": pair}).wait_recv()
+            rdma(crossed, crossed, rs.at[0, cc], rr.at[cc], {"fs": pair}).wait_recv()
+            mixed[:, cc * chunk:(cc + 1) * chunk] = (
+                part[t * per_owner + cc, z].astype(jnp.float32)
+                + ret[0, cc].astype(jnp.float32)
+                + ret[1, cc].astype(jnp.float32)
+            ).astype(jnp.bfloat16)
+
+    final()
+
+    def send_waits():
+        @pl.loop(1, nz)
+        def _(k):
+            rdma(wsend.at[to(k)], wrecv.at[z], gs.at[k], gr.at[k], {"fs": to(k)}).wait_send()
+            for m in range(2):
+                zd_copy(m, k).wait_send()
+                relay(dpiece(m, g, frm(k)), m, nb, k).wait_send()
+            token_quarter(2, frm(k), over).wait_send()
+
+            @pl.loop(0, nb)
+            def _(b):
+                for m in range(2):
+                    z_copy(m, b, k).wait_send()
+                    relay(piece(m, b, g, frm(k)), m, b, k).wait_send()
+
         for m in range(2):
-            zd_copy(m, k).wait_send()
-            relay(dpiece(m, g, frm(k)), m, nb, k).wait_send()
-        token_quarter(2, frm(k), over).wait_send()
-
-        @pl.loop(0, nb)
-        def _(b):
-            for m in range(2):
-                z_copy(m, b, k).wait_send()
-                relay(piece(m, b, g, frm(k)), m, b, k).wait_send()
-
-    for m in range(2):
-        xd_own(m).wait_send()
-
-        @pl.loop(0, nb)
-        def _(b):
-            x_own(m, b).wait_send()
-
-    for flag, c in guarded:
-        @pl.when(flag)
-        def _(c=c):
-            c.wait_send()
-
-    @pl.loop(0, n)
-    def _(i):
-        k, other, c, owner, par, yo, cc = chunk_of(i)
-
-        @pl.when(par != core)
-        def _():
-            give(i).wait_send()
-
-        @pl.when(jnp.logical_and(par == core, yo != y))
-        def _():
-            for j in range(nz):
-                up(i, j).wait_send()
-
-    for cc in range(per_owner):
-        c = t * per_owner + cc
-        near(c, cc, 2).wait_send()
-        for j in range(2):
-            @pl.when(inner)
-            def _(j=j, cc=cc):
-                cross(cc, j).wait_send()
-
-            @pl.when(jnp.logical_not(inner))
-            def _(j=j, c=c, cc=cc):
-                near(c, cc, j).wait_send()
+            xd_own(m).wait_send()
+
+            @pl.loop(0, nb)
+            def _(b):
+                x_own(m, b).wait_send()
+
+        for flag, c in guarded:
+            @pl.when(flag)
+            def _(c=c):
+                c.wait_send()
+
+        @pl.loop(0, n)
+        def _(i):
+            k, other, c, owner, par, yo, cc = chunk_of(i)
+
+            @pl.when(par != core)
+            def _():
+                for j in range(nz):
+                    give(i, j).wait_send()
+
+            @pl.when(jnp.logical_and(par == core, yo != y))
+            def _():
+                for j in range(nz):
+                    up(i, j).wait_send()
+
+        for cc in range(per_owner):
+            c = t * per_owner + cc
+            near(c, cc, 2).wait_send()
+            for j in range(2):
+                @pl.when(inner)
+                def _(j=j, cc=cc):
+                    cross(cc, j).wait_send()
+
+                @pl.when(jnp.logical_not(inner))
+                def _(j=j, c=c, cc=cc):
+                    near(c, cc, j).wait_send()
+
+    send_waits()
 
 
 def store(gate, upper, down, mixed, gate_out, up_out, down_out, mixed_out, sem):
@@ -483,7 +540,7 @@
             dma((nz,)), dma((nz,)),
             dma((2, BLOCKS + 1, nz)), dma((2, BLOCKS + 1, nz)),
             dma((2, BLOCKS + 1, nz)), dma((2, BLOCKS + 1, nz)),
-            dma((chunks,)), dma((chunks,)),
+            dma((chunks, nz)), dma((chunks, nz)),
             dma((chunks, nz)), dma((chunks, nz)),
             dma((3, per_owner)), dma((3, per_owner)),
             dma((2, per_owner)), dma((per_owner,)),

time: 254 us -> 220 us (0.87); the launches traced: 251 us -> 220 us
  Pallas kernels: 250 us -> 219 us
    pallas_call x1, Pallas kernels: 245 us -> 215 us  [fused(): pl.pallas_call(functools.partial(kernel, ng, nz, nt), out_shape=(full, fu...]
where the time goes in v2:
time: 220 us
  Pallas kernels  219 us (100%)
    pallas_call x1, Pallas kernels, fused(): pl.pallas_call(functools.partial(kernel, ng, nz, nt), out_shape=(full, fu...  215 us
    pallas_call x1, Pallas kernels, fused(): pl.pallas_call(store, out_shape=(whole, whole, whole, jax.ShapeDtypeStruc...  4.73 us

profile of v2, /device:TPU:12, one launch (start us, length us, event | category | flops | bytes accessed | tf_op | source)
XLA Modules:
  0.0 220.0 jit_solution(6285512632268271673)
XLA Ops:
  0.6 214.6 %shard_map.102 = (bf16[2048,1024]{1,0:T(8,128)(2,1)S(1)}, bf16[2048,1024]{1,0:T(8,128)(2,1)S(1)}, bf16[2048,1024]{1,0:T(8,128)(2,1)S(1)}, bf16[512,512]{1,0:T(8,128)(2,1)S(1)}) custom-call(bf16[512,2048]{1,0:T(8,128)(2,1)} %tok_in.1, s32[2,512]{1,0:T(2,128)} %bitcast.3, f32[2,512]{1,0:T(2,128)} %bitcast.4, f32[1,256]{1,0:T(1,128)} %bitcast.5, ...), custom_call_target="tpu_custom_call" | custom-call | tf_op jit(solution)/shard_map/pallas_call | solution.py:518
  215.2 4.7 %shard_map.103 = (bf16[1,2048,1024]{2,1,0:T(8,128)(2,1)}, bf16[1,2048,1024]{2,1,0:T(8,128)(2,1)}, bf16[1,2048,1024]{2,1,0:T(8,128)(2,1)}, bf16[512,512]{1,0:T(8,128)(2,1)}) custom-call(bf16[2048,1024]{1,0:T(8,128)(2,1)S(1)} %get-tuple-element.8.gate, bf16[2048,1024]{1,0:T(8,128)(2,1)S(1)} %get-tuple-element.9.upper, ...), custom_call_target="tpu_custom_call" | custom-call | tf_op jit(solution)/shard_map/pallas_call | solution.py:553

commit v3 on v2

--- a/solution.py
+++ b/solution.py
@@ -89,8 +89,8 @@
             z_arrive(ref, m, b, k)
             relay(ref, m, b, k).start()
 
-    def zd_take(k):
-        for m in range(2):
+    def zd_take(k, ms=(0, 1)):
+        for m in ms:
             ref = dpiece(m, g, frm(k))
             z_arrive(ref, m, nb, k)
             relay(ref, m, nb, k).start()
@@ -101,9 +101,9 @@
     def k_of(s):
         return jnp.where(s == 0, 0, jnp.where(s == 1, k_near, jnp.where(s == 2, k_far, k_mid)))
 
-    def z_cross(b):
-        for k in (2, k_near):
-            for m in range(2):
+    def z_cross(b, ms=(0, 1)):
+        for m in ms:
+            for k in (2, k_near):
                 z_copy(m, b, k).start()
 
     def z_side(b):
@@ -111,8 +111,10 @@
             z_copy(m, b, near_to).start()
 
     def z_down():
-        for k in (near_to, 2, k_near):
-            for m in range(2):
+        for m in range(2):
+            zd_copy(m, near_to).start()
+        for m in range(2):
+            for k in (2, k_near):
                 zd_copy(m, k).start()
 
     load_tok = pltpu.make_async_copy(tok_in, raw, ld.at[0])
@@ -187,6 +189,7 @@
     @pl.when(inner)
     def _():
         z_side(0)
+        z_cross(0, (0,))
 
     for b in range(nb):
         for m in range(2):
@@ -226,7 +229,7 @@
 
     @pl.when(inner)
     def _():
-        z_cross(0)
+        z_cross(0, (1,))
         take_near(0, nb // 2)
     hops(2)
 
@@ -313,24 +316,37 @@
         owner = c // per_owner
         return k, other, c, owner, lax.rem(owner, 2), owner // 2, lax.rem(c, per_owner)
 
-    def give(i, j):
+    def cut(ref, h):
+        return ref if h is None else ref.at[:, pl.ds(h * half, half)]
+
+    def slot_of(i, h):
+        return i + 2 if h == 1 else i
+
+    def give(i, j, h):
         k, other, c, owner, par, yo, cc = chunk_of(i)
-        b = order_of(j)
-        return rdma(part.at[c, b], crx.at[yo * per_owner + cc, b], cs.at[i, j], cr.at[i, j], {"tp": mate})
-
-    def up(i, j):
+        b, si = order_of(j), slot_of(i, h)
+        src, dst = cut(part.at[c, b], h), cut(crx.at[yo * per_owner + cc, b], h)
+        return rdma(src, dst, cs.at[si, j], cr.at[si, j], {"tp": mate})
+
+    def up(i, j, h):
         k, other, c, owner, par, yo, cc = chunk_of(i)
-        return rdma(part.at[c, order[j]], yrx.at[cc, order[j]], ys.at[i, j], yr.at[i, j], {"tp": over})
-
-    def near(c, cc, j):
+        si = slot_of(i, h)
+        src, dst = cut(part.at[c, order[j]], h), cut(yrx.at[cc, order[j]], h)
+        return rdma(src, dst, ys.at[si, j], yr.at[si, j], {"tp": over})
+
+    def near(c, cc, j, h):
+        second = 1 if h == 1 else 0
         dst = rly.at[j, cc] if j < 2 else ret.at[0, cc]
-        return rdma(part.at[c, order[j]], dst, hs.at[j, cc], hr.at[j, cc], {"fs": pair})
-
-    def cross(cc, j):
-        return rdma(part.at[t * per_owner + cc, order[j]], ret.at[1, cc], rs.at[j, cc], rr.at[cc], {"fs": order[j]})
-
-    def x_down_wait(k):
-        for m in range(2):
+        landed = hr.at[j, cc, second if j < 2 else 0]
+        return rdma(cut(part.at[c, order[j]], h), cut(dst, h), hs.at[j, cc, second], landed, {"fs": pair})
+
+    def cross(cc, j, h):
+        second = 1 if h == 1 else 0
+        src, dst = cut(part.at[t * per_owner + cc, order[j]], h), cut(ret.at[1, cc], h)
+        return rdma(src, dst, rs.at[j, cc, second], rr.at[cc], {"fs": order[j]})
+
+    def x_down_wait(k, ms):
+        for m in ms:
             ref = dpiece(m, 1 - g, frm(k))
             rdma(ref, ref, xs.at[m, nb, k], xr.at[m, nb, k], {"gr": 1 - g}).wait_recv()
 
@@ -339,8 +355,7 @@
 
         @pl.when(other == 1)
         def _():
-            x_down_wait(k)
-
+            x_down_wait(k, range(2))
         mine = pl.ds(pl.multiple_of(c * chunk, chunk), chunk)
 
         @pl.loop(0, nz)
@@ -352,81 +367,130 @@
 
             @pl.when(par != core)
             def _():
-                give(i, j).start()
-
-    def stage_b(i):
+                give(i, j, None).start()
+
+    def halves_a(i, h):
         k, other, c, owner, par, yo, cc = chunk_of(i)
+        c2 = chunk_of(i + 1)[2]
+        x_down_wait(k, (h,))
+        mine = [pl.ds(pl.multiple_of(v * chunk + h * half, half), half) for v in (c, c2)]
+
+        @pl.loop(0, nz)
+        def _(j):
+            b = order_of(j)
+            both = lax.dot_general(
+                hid[b], jnp.concatenate([dout[v, :] for v in mine], axis=0), (((1,), (1,)), ((), ())),
+                preferred_element_type=jnp.float32,
+            ).astype(jnp.bfloat16)
+            cut(part.at[c, b], h)[...] = both[:, :half]
+            cut(part.at[c2, b], h)[...] = both[:, half:]
+
+            @pl.when(par != core)
+            def _():
+                give(i, j, h).start()
+                give(i + 1, j, h).start()
+
+    def add(c, b, h, ref):
+        mine = cut(part.at[c, b], h)
+        mine[...] = (mine[...].astype(jnp.float32) + ref[...].astype(jnp.float32)).astype(jnp.bfloat16)
+
+    def stage_b(i, h=None):
+        k, other, c, owner, par, yo, cc = chunk_of(i)
+        si = slot_of(i, h)
 
         @pl.when(par == core)
         def _():
             for j in range(nz):
                 b = order[j]
-                slot = crx.at[yo * per_owner + cc, b]
-                rdma(slot, slot, cs.at[i, j], cr.at[i, j], {"tp": mate}).wait_recv()
-                part[c, b] = (
-                    part[c, b].astype(jnp.float32) + crx[yo * per_owner + cc, b].astype(jnp.float32)
-                ).astype(jnp.bfloat16)
+                ref = cut(crx.at[yo * per_owner + cc, b], h)
+                rdma(ref, ref, cs.at[si, j], cr.at[si, j], {"tp": mate}).wait_recv()
+                add(c, b, h, ref)
 
                 @pl.when(yo != y)
                 def _(j=j):
-                    up(i, j).start()
-
-    def stage_c(i):
+                    up(i, j, h).start()
+
+    def stage_c(i, h=None):
         k, other, c, owner, par, yo, cc = chunk_of(i)
+        si = slot_of(i, h)
 
         @pl.when(owner == t)
         def _():
             for j in range(nz):
                 b = order[j]
-                slot = yrx.at[cc, b]
-                rdma(slot, slot, ys.at[i, j], yr.at[i, j], {"tp": over}).wait_recv()
-                part[c, b] = (
-                    part[c, b].astype(jnp.float32) + yrx[cc, b].astype(jnp.float32)
-                ).astype(jnp.bfloat16)
+                ref = cut(yrx.at[cc, b], h)
+                rdma(ref, ref, ys.at[si, j], yr.at[si, j], {"tp": over}).wait_recv()
+                add(c, b, h, ref)
                 if j < 2:
                     @pl.when(jnp.logical_not(inner))
                     def _(j=j):
-                        near(c, cc, j).start()
+                        near(c, cc, j, h).start()
                 elif j == 2:
-                    near(c, cc, j).start()
+                    near(c, cc, j, h).start()
+
+    def cross_phase(cc, h=None):
+        for j in range(2):
+            ref = cut(rly.at[j, cc], h)
+            rdma(ref, ref, hs.at[j, cc, 0], hr.at[j, cc, 1 if h == 1 else 0], {"fs": pair}).wait_recv()
+            add(t * per_owner + cc, order[j], h, ref)
+            cross(cc, j, h).start()
 
     n = chunks
-
-    @pl.loop(0, n + LAG)
+    early = jnp.logical_and(inner, side == core)
+    late = jnp.logical_and(inner, side != core)
+    cc_far = lax.rem(frm(k_far), 2)
+    zd_take(k_near)
+
+    @pl.loop(0, n - 2)
     def _(i):
-        @pl.when(jnp.logical_or(i == 2, jnp.logical_or(i == 3, i == 5)))
-        def _():
-            zd_take(k_of((i + 1) // 2))
-
-        @pl.when(i < n)
-        def _():
-            stage_a(i)
-            stage_b(i)
-
-        @pl.when(i >= LAG)
-        def _():
-            stage_c(i - LAG)
-
-    def cross_phase():
-        first = jnp.where(side == core, 0, 1)
-        for turn in range(per_owner):
-            cc = first + turn * (1 - 2 * first)
-            for j in range(2):
-                slot = rly.at[j, cc]
-                rdma(slot, slot, hs.at[j, cc], hr.at[j, cc], {"fs": pair}).wait_recv()
-                c, b = t * per_owner + cc, order[j]
-                part[c, b] = (
-                    part[c, b].astype(jnp.float32) + rly[j, cc].astype(jnp.float32)
-                ).astype(jnp.bfloat16)
-                cross(cc, j).start()
-
-    pl.when(inner)(cross_phase)
+        @pl.when(i == 2)
+        def _():
+            zd_take(k_far, (0,))
+
+        @pl.when(i == 4)
+        def _():
+            zd_take(k_far, (1,))
+            pl.loop(0, 2)(stage_c)
+            zd_take(k_mid, (0,))
+
+        stage_a(i)
+        stage_b(i)
+
+    pl.loop(2, 4)(stage_c)
+
+    def last(h):
+        halves_a(n - 2, h)
+
+        @pl.loop(n - 2, n)
+        def _(i):
+            stage_b(i, h)
+
+    last(0)
+    zd_take(k_mid, (1,))
+
+    @pl.when(early)
+    def _():
+        pl.loop(0, per_owner)(cross_phase)
+    pl.loop(n - 4, n - 2)(stage_c)
+    last(1)
+
+    @pl.when(late)
+    def _():
+        cross_phase(cc_far)
+    for h in range(2):
+        @pl.loop(n - 2, n)
+        def _(i, h=h):
+            stage_c(i, h)
+
+        @pl.when(late)
+        def _(h=h):
+            cross_phase(1 - cc_far, h)
 
     def final():
         for cc in range(per_owner):
             direct, crossed = ret.at[0, cc], ret.at[1, cc]
-            rdma(direct, direct, hs.at[2, cc], hr.at[2, cc], {"fs": pair}).wait_recv()
-            rdma(crossed, crossed, rs.at[0, cc], rr.at[cc], {"fs": pair}).wait_recv()
+            rdma(direct, direct, hs.at[2, cc, 0], hr.at[2, cc, 0], {"fs": pair}).wait_recv()
+            rdma(crossed, crossed, rs.at[0, cc, 0], rr.at[cc], {"fs": pair}).wait_recv()
             mixed[:, cc * chunk:(cc + 1) * chunk] = (
                 part[t * per_owner + cc, z].astype(jnp.float32)
                 + ret[0, cc].astype(jnp.float32)
@@ -462,31 +526,48 @@
             def _(c=c):
                 c.wait_send()
 
-        @pl.loop(0, n)
-        def _(i):
+        def sent(i, h):
             k, other, c, owner, par, yo, cc = chunk_of(i)
 
             @pl.when(par != core)
             def _():
                 for j in range(nz):
-                    give(i, j).wait_send()
+                    give(i, j, h).wait_send()
 
             @pl.when(jnp.logical_and(par == core, yo != y))
             def _():
                 for j in range(nz):
-                    up(i, j).wait_send()
-
-        for cc in range(per_owner):
+                    up(i, j, h).wait_send()
+
+        def returned(cc, h):
             c = t * per_owner + cc
-            near(c, cc, 2).wait_send()
+            near(c, cc, 2, h).wait_send()
             for j in range(2):
                 @pl.when(inner)
-                def _(j=j, cc=cc):
-                    cross(cc, j).wait_send()
+                def _(j=j):
+                    cross(cc, j, h).wait_send()
 
                 @pl.when(jnp.logical_not(inner))
-                def _(j=j, c=c, cc=cc):
-                    near(c, cc, j).wait_send()
+                def _(j=j):
+                    near(c, cc, j, h).wait_send()
+
+        @pl.loop(0, n - 2)
+        def _(i):
+            sent(i, None)
+        for h in range(2):
+            @pl.loop(n - 2, n)
+            def _(i, h=h):
+                sent(i, h)
+        returned(cc_far, None)
+
+        @pl.when(side == core)
+        def _():
+            returned(1 - cc_far, None)
+
+        @pl.when(side != core)
+        def _():
+            for h in range(2):
+                returned(1 - cc_far, h)
 
     send_waits()
 
@@ -540,10 +621,10 @@
             dma((nz,)), dma((nz,)),
             dma((2, BLOCKS + 1, nz)), dma((2, BLOCKS + 1, nz)),
             dma((2, BLOCKS + 1, nz)), dma((2, BLOCKS + 1, nz)),
-            dma((chunks, nz)), dma((chunks, nz)),
-            dma((chunks, nz)), dma((chunks, nz)),
-            dma((3, per_owner)), dma((3, per_owner)),
-            dma((2, per_owner)), dma((per_owner,)),
+            dma((chunks + 2, nz)), dma((chunks + 2, nz)),
+            dma((chunks + 2, nz)), dma((chunks + 2, nz)),
+            dma((3, per_owner, 2)), dma((3, per_owner, 2)),
+            dma((2, per_owner, 2)), dma((per_owner,)),
         ],
         compiler_params=pltpu.CompilerParams(
             collective_id=0, has_side_effects=True, vmem_limit_bytes=VMEM_LIMIT

time: 220 us -> 204 us (0.927)
  Pallas kernels: 219 us -> 202 us
    pallas_call x1, Pallas kernels: 215 us -> 197 us  [fused(): pl.pallas_call(functools.partial(kernel, ng, nz, nt), out_shape=(full, fu...]
where the time goes in v3:
time: 204 us; the launch traced here: 203 us
  Pallas kernels  202 us (99%)
    pallas_call x1, Pallas kernels, fused(): pl.pallas_call(functools.partial(kernel, ng, nz, nt), out_shape=(full, fu...  197 us
    pallas_call x1, Pallas kernels, fused(): pl.pallas_call(store, out_shape=(whole, whole, whole, jax.ShapeDtypeStruc...  4.73 us

profile of v3, /device:TPU:12, one launch (start us, length us, event | category | flops | bytes accessed | tf_op | source)
XLA Modules:
  0.0 202.8 jit_solution(2509177870403212368)
XLA Ops:
  0.6 197.4 %shard_map.102 = (bf16[2048,1024]{1,0:T(8,128)(2,1)S(1)}, bf16[2048,1024]{1,0:T(8,128)(2,1)S(1)}, bf16[2048,1024]{1,0:T(8,128)(2,1)S(1)}, bf16[512,512]{1,0:T(8,128)(2,1)S(1)}) custom-call(bf16[512,2048]{1,0:T(8,128)(2,1)} %tok_in.1, s32[2,512]{1,0:T(2,128)} %bitcast.3, f32[2,512]{1,0:T(2,128)} %bitcast.4, f32[1,256]{1,0:T(1,128)} %bitcast.5, ...), custom_call_target="tpu_custom_call" | custom-call | tf_op jit(solution)/shard_map/pallas_call | solution.py:599
  198.0 4.7 %shard_map.103 = (bf16[1,2048,1024]{2,1,0:T(8,128)(2,1)}, bf16[1,2048,1024]{2,1,0:T(8,128)(2,1)}, bf16[1,2048,1024]{2,1,0:T(8,128)(2,1)}, bf16[512,512]{1,0:T(8,128)(2,1)}) custom-call(bf16[2048,1024]{1,0:T(8,128)(2,1)S(1)} %get-tuple-element.8.gate, bf16[2048,1024]{1,0:T(8,128)(2,1)S(1)} %get-tuple-element.9.upper, ...), custom_call_target="tpu_custom_call" | custom-call | tf_op jit(solution)/shard_map/pallas_call | solution.py:634

commit v4 on v3

--- a/solution.py
+++ b/solution.py
@@ -14,7 +14,7 @@
 
 
 def kernel(ng, nz, nt, tok_in, routes, rweight, gain, gw, uw, dw, gout, uout, dout, mixed,
-           tok, hid, part, crx, yrx, stage, raw, ret, rly, wsend, wrecv, wcol, gcol,
+           tok, packed, hid, part, crx, yrx, full, stage, raw, ret, rly, wsend, wrecv, wcol, gcol, before, pick, spread,
            ld, ts, tr, fs_s, fr, gs, gr, zs, zr, xs, xr, cs, cr, ys, yr, hs, hr, rs, rr):
     g, z, t = lax.axis_index("gr"), lax.axis_index("fs"), lax.axis_index("tp")
     core, y = lax.rem(t, 2), lax.div(t, 2)
@@ -22,6 +22,7 @@
     quarter = d // nt
     chunk, width = gw.shape[1], gw.shape[2]
     half = chunk // 2
+    cap = packed.shape[1]
     chunks = ng * nz
     per_owner = chunks // nt
     nb = BLOCKS
@@ -110,9 +111,11 @@
         for m in range(2):
             z_copy(m, b, near_to).start()
 
-    def z_down():
+    def z_down_side():
         for m in range(2):
             zd_copy(m, near_to).start()
+
+    def z_down_cross():
         for m in range(2):
             for k in (2, k_near):
                 zd_copy(m, k).start()
@@ -162,39 +165,6 @@
         return rdma(ref, ref, ts.at[(way + 1) // 2, h], tr.at[src], {"fs": nxt})
 
     right, left = z + 1 < nz, z >= 1
-    guard(right, hop(1, 0, z))
-    guard(left, hop(-1, 0, z))
-    for m in range(2):
-        xd_own(m).start()
-
-    def scaleall():
-        gcol[...] = jnp.transpose(jnp.broadcast_to(gain[...], (128, chunk)))
-        for c in loads:
-            c.wait()
-
-        @pl.loop(0, nz * (chunk // step))
-        def _(i):
-            e = i // (chunk // step)
-            at = pl.ds(pl.multiple_of(lax.rem(i, chunk // step) * step, step), step)
-            factor = jnp.concatenate([gcol[at, :]] * (width // 128), axis=1)
-            for m in range(2):
-                stage[m, e, at, :] = (stage[m, e, at, :].astype(jnp.float32) * factor).astype(jnp.bfloat16)
-
-    scaleall()
-    @pl.when(jnp.logical_not(inner))
-    def _():
-        pl.loop(0, nb)(z_side)
-        pl.loop(0, nb)(z_cross)
-
-    @pl.when(inner)
-    def _():
-        z_side(0)
-        z_cross(0, (0,))
-
-    for b in range(nb):
-        for m in range(2):
-            x_own(m, b).start()
-
     for e in range(nz):
         wsend[e] = (
             jnp.where(routes[0:1, :] == e, rweight[0:1, :], 0.0)
@@ -203,8 +173,44 @@
     wrecv[z] = wsend[z]
     for k in range(1, nz):
         rdma(wsend.at[to(k)], wrecv.at[z], gs.at[k], gr.at[k], {"fs": to(k)}).start()
+    guard(right, hop(1, 0, z))
+    guard(left, hop(-1, 0, z))
+    for m in range(2):
+        xd_own(m).start()
+
+    def scaleall():
+        gcol[...] = jnp.transpose(jnp.broadcast_to(gain[...], (128, chunk)))
+        for c in loads:
+            c.wait()
+
+        @pl.loop(0, nz * (chunk // step))
+        def _(i):
+            e = i // (chunk // step)
+            at = pl.ds(pl.multiple_of(lax.rem(i, chunk // step) * step, step), step)
+            factor = jnp.concatenate([gcol[at, :]] * (width // 128), axis=1)
+            for m in range(2):
+                stage[m, e, at, :] = (stage[m, e, at, :].astype(jnp.float32) * factor).astype(jnp.bfloat16)
+
+    scaleall()
+    @pl.when(jnp.logical_not(inner))
+    def _():
+        pl.loop(0, nb)(z_side)
+        pl.loop(0, nb)(z_cross)
+
+    @pl.when(inner)
+    def _():
+        z_side(0)
+        z_cross(0, (0,))
+
+    for b in range(nb):
+        for m in range(2):
+            x_own(m, b).start()
+
     for m in range(2):
         outs[m][own_rows, :] = stage[m, z]
+    before[...] = jnp.where(
+        lax.broadcasted_iota(jnp.int32, (rows, rows), 0) < lax.broadcasted_iota(jnp.int32, (rows, rows), 1), 1.0, 0.0
+    ).astype(jnp.bfloat16)
 
     def hops(h):
         for way in (1, -1):
@@ -220,41 +226,110 @@
             guard(valid, rdma(ref, ref, fs_s.at[1, src], fr.at[1, src], {"tp": over}))
             guard(valid, rdma(ref, ref, fs_s.at[0, src], fr.at[0, src], {"tp": mate}))
 
+    def token_quarter(lane, src, q):
+        ref = tok.at[src, :, qcols(q)]
+        return rdma(ref, ref, fs_s.at[lane, src], fr.at[lane, src], {"tp": mate})
+
+    def forward(s):
+        src = frm(k_of(s))
+        token_quarter(1, src, over).wait_recv()
+        token_quarter(2, src, over).start()
+
+    def tok_wait(src, s):
+        token_quarter(0, src, mate).wait_recv()
+        token_quarter(2, src, (1 - y) * 2 + 1 - core).wait_recv()
+        rdma(wrecv.at[src], wrecv.at[src], gs.at[s], gr.at[s], {"fs": to(s)}).wait_recv()
+
+    def prepare(s):
+        src = frm(k_of(s))
+
+        @pl.when(s >= 1)
+        def _():
+            tok_wait(src, k_of(s))
+        weight = wrecv[src]
+        chosen = weight != 0.0
+        marks = jnp.broadcast_to(jnp.where(chosen, 1.0, 0.0), (16, rows)).astype(jnp.bfloat16)
+        rank = jnp.dot(marks, before[...], preferred_element_type=jnp.float32)[0:1]
+        key = jnp.where(chosen, rank, -1.0)
+        match = key == lax.broadcasted_iota(jnp.int32, (cap, rows), 0).astype(jnp.float32)
+        own_weight = jnp.sum(jnp.where(match, weight, 0.0), axis=1, keepdims=True)
+        wcol[src] = jnp.broadcast_to(own_weight, (cap, 128))
+        pick[...] = jnp.where(match, 1.0, 0.0).astype(jnp.bfloat16)
+        column = jnp.transpose(jnp.broadcast_to(key, (128, rows)))
+        lane = lax.broadcasted_iota(jnp.int32, (rows, 128), 1).astype(jnp.float32)
+        for v in range(cap // 128):
+            spread[src, :, v * 128:(v + 1) * 128] = jnp.where(column == lane + v * 128.0, 1.0, 0.0).astype(jnp.bfloat16)
+
+        @pl.loop(0, nt)
+        def _(q):
+            packed[src, :, qcols(q)] = jnp.dot(
+                pick[...], tok[src, :, qcols(q)], preferred_element_type=jnp.float32
+            ).astype(jnp.bfloat16)
+
     def take_near(lo, hi):
         @pl.loop(lo, hi)
         def _(b):
             z_take(b, k_near)
 
+    ends = jnp.logical_not(inner)
     hops(1)
 
     @pl.when(inner)
     def _():
         z_cross(0, (1,))
         take_near(0, nb // 2)
+
+    @pl.when(ends)
+    def _():
+        z_take(0, k_near)
     hops(2)
 
     @pl.when(inner)
     def _():
         pl.loop(1, nb)(z_side)
         pl.loop(1, nb)(z_cross)
-        z_down()
+        z_down_side()
+        z_down_cross()
         take_near(nb // 2, nb)
+
+    @pl.when(ends)
+    def _():
+        z_take(0, k_far)
     for h in range(3, nz):
         hops(h)
-
-    z_take(0, k_mid)
+    for s in (1, 3):
+        forward(s)
+
+    @pl.when(inner)
+    def _():
+        forward(2)
+    pl.loop(0, 2)(prepare)
 
     @pl.loop(0, nb)
     def _(b):
-        z_take(b, k_far)
-
-        @pl.when(jnp.logical_and(jnp.logical_not(inner), lax.rem(b, 2) == 0))
-        def _():
-            z_take(b // 2, k_near)
-
-    def token_quarter(lane, src, q):
-        ref = tok.at[src, :, qcols(q)]
-        return rdma(ref, ref, fs_s.at[lane, src], fr.at[lane, src], {"tp": mate})
+        @pl.when(jnp.logical_or(inner, b >= 1))
+        def _():
+            z_take(b, k_far)
+
+        @pl.when(jnp.logical_and(ends, lax.rem(b, 2) == 1))
+        def _():
+            z_take(b // 2 + 1, k_near)
+
+        @pl.when(b == 0)
+        def _():
+            prepare(3)
+
+            @pl.when(ends)
+            def _():
+                forward(2)
+
+        @pl.when(b == 1)
+        def _():
+            prepare(2)
+
+        @pl.when(b == nb // 2)
+        def _():
+            z_take(0, k_mid)
 
     def x_wait(b):
         @pl.loop(0, nz)
@@ -263,15 +338,8 @@
                 ref = piece(m, b, 1 - g, frm(kk))
                 rdma(ref, ref, xs.at[m, b, kk], xr.at[m, b, kk], {"gr": 1 - g}).wait_recv()
 
-    def tok_wait(src, s):
-        token_quarter(1, src, over).wait_recv()
-        token_quarter(2, src, over).start()
-        token_quarter(0, src, mate).wait_recv()
-        token_quarter(2, src, (1 - y) * 2 + 1 - core).wait_recv()
-        rdma(wrecv.at[src], wrecv.at[src], gs.at[s], gr.at[s], {"fs": to(s)}).wait_recv()
-
     def hidden(b, src):
-        a = tok[src]
+        a = packed[src]
         gate = jnp.dot(a, gout[:, cols(b)], preferred_element_type=jnp.float32)
         upper = jnp.dot(a, uout[:, cols(b)], preferred_element_type=jnp.float32)
         weight = jnp.concatenate([wcol[src]] * (blk // 128), axis=1)
@@ -286,24 +354,22 @@
         def _():
             z_take(b, k_mid)
 
-        @pl.when(jnp.logical_and(jnp.logical_not(inner), jnp.logical_and(s == 1, b < (nb + 1) // 2 + 1)))
-        def _():
-            z_take(b + nb // 2 - 1, k_near)
-
-        @pl.when(jnp.logical_and(jnp.logical_not(inner), i == (nb - 1) * nz))
-        def _():
-            z_down()
+        @pl.when(jnp.logical_and(jnp.logical_not(inner), jnp.logical_and(s == 1, b < nb - nb // 2)))
+        def _():
+            z_take(b + nb // 2, k_near)
+
+        @pl.when(jnp.logical_and(jnp.logical_not(inner), i == (nb - 2) * nz))
+        def _():
+            z_down_side()
+
+        @pl.when(jnp.logical_and(jnp.logical_not(inner), i == nb * nz))
+        def _():
+            z_down_cross()
+            zd_take(k_near)
 
         @pl.when(s == 0)
         def _():
             x_wait(b - 1)
-
-        @pl.when(b == 1)
-        def _():
-            @pl.when(s >= 1)
-            def _():
-                tok_wait(src, k_of(s))
-            wcol[src] = jnp.transpose(jnp.broadcast_to(wrecv[src], (128, rows)))
 
         hidden(b - 1, src)
 
@@ -334,15 +400,15 @@
         src, dst = cut(part.at[c, order[j]], h), cut(yrx.at[cc, order[j]], h)
         return rdma(src, dst, ys.at[si, j], yr.at[si, j], {"tp": over})
 
-    def near(c, cc, j, h):
+    def near(cc, j, h):
         second = 1 if h == 1 else 0
         dst = rly.at[j, cc] if j < 2 else ret.at[0, cc]
         landed = hr.at[j, cc, second if j < 2 else 0]
-        return rdma(cut(part.at[c, order[j]], h), cut(dst, h), hs.at[j, cc, second], landed, {"fs": pair})
+        return rdma(cut(full.at[cc, order[j]], h), cut(dst, h), hs.at[j, cc, second], landed, {"fs": pair})
 
     def cross(cc, j, h):
         second = 1 if h == 1 else 0
-        src, dst = cut(part.at[t * per_owner + cc, order[j]], h), cut(ret.at[1, cc], h)
+        src, dst = cut(full.at[cc, order[j]], h), cut(ret.at[1, cc], h)
         return rdma(src, dst, rs.at[j, cc, second], rr.at[cc], {"fs": order[j]})
 
     def x_down_wait(k, ms):
@@ -390,8 +456,8 @@
                 give(i, j, h).start()
                 give(i + 1, j, h).start()
 
-    def add(c, b, h, ref):
-        mine = cut(part.at[c, b], h)
+    def add(target, h, ref):
+        mine = cut(target, h)
         mine[...] = (mine[...].astype(jnp.float32) + ref[...].astype(jnp.float32)).astype(jnp.bfloat16)
 
     def stage_b(i, h=None):
@@ -404,7 +470,7 @@
                 b = order[j]
                 ref = cut(crx.at[yo * per_owner + cc, b], h)
                 rdma(ref, ref, cs.at[si, j], cr.at[si, j], {"tp": mate}).wait_recv()
-                add(c, b, h, ref)
+                add(part.at[c, b], h, ref)
 
                 @pl.when(yo != y)
                 def _(j=j):
@@ -420,26 +486,32 @@
                 b = order[j]
                 ref = cut(yrx.at[cc, b], h)
                 rdma(ref, ref, ys.at[si, j], yr.at[si, j], {"tp": over}).wait_recv()
-                add(c, b, h, ref)
+                total = cut(part.at[c, b], h)[...].astype(jnp.float32) + ref[...].astype(jnp.float32)
+                cut(full.at[cc, b], h)[...] = jnp.dot(
+                    spread[b], total.astype(jnp.bfloat16), preferred_element_type=jnp.float32
+                ).astype(jnp.bfloat16)
                 if j < 2:
                     @pl.when(jnp.logical_not(inner))
                     def _(j=j):
-                        near(c, cc, j, h).start()
+                        near(cc, j, h).start()
                 elif j == 2:
-                    near(c, cc, j, h).start()
+                    near(cc, j, h).start()
 
     def cross_phase(cc, h=None):
         for j in range(2):
             ref = cut(rly.at[j, cc], h)
             rdma(ref, ref, hs.at[j, cc, 0], hr.at[j, cc, 1 if h == 1 else 0], {"fs": pair}).wait_recv()
-            add(t * per_owner + cc, order[j], h, ref)
+            add(full.at[cc, order[j]], h, ref)
             cross(cc, j, h).start()
 
     n = chunks
     early = jnp.logical_and(inner, side == core)
     late = jnp.logical_and(inner, side != core)
     cc_far = lax.rem(frm(k_far), 2)
-    zd_take(k_near)
+
+    @pl.when(inner)
+    def _():
+        zd_take(k_near)
 
     @pl.loop(0, n - 2)
     def _(i):
@@ -451,11 +523,11 @@
         def _():
             zd_take(k_far, (1,))
             pl.loop(0, 2)(stage_c)
-            zd_take(k_mid, (0,))
 
         stage_a(i)
         stage_b(i)
 
+    zd_take(k_mid, (0,))
     pl.loop(2, 4)(stage_c)
 
     def last(h):
@@ -472,11 +544,11 @@
     def _():
         pl.loop(0, per_owner)(cross_phase)
     pl.loop(n - 4, n - 2)(stage_c)
+
+    @pl.when(late)
+    def _():
+        cross_phase(cc_far)
     last(1)
-
-    @pl.when(late)
-    def _():
-        cross_phase(cc_far)
     for h in range(2):
         @pl.loop(n - 2, n)
         def _(i, h=h):
@@ -492,7 +564,7 @@
             rdma(direct, direct, hs.at[2, cc, 0], hr.at[2, cc, 0], {"fs": pair}).wait_recv()
             rdma(crossed, crossed, rs.at[0, cc, 0], rr.at[cc], {"fs": pair}).wait_recv()
             mixed[:, cc * chunk:(cc + 1) * chunk] = (
-                part[t * per_owner + cc, z].astype(jnp.float32)
+                full[cc, z].astype(jnp.float32)
                 + ret[0, cc].astype(jnp.float32)
                 + ret[1, cc].astype(jnp.float32)
             ).astype(jnp.bfloat16)
@@ -540,8 +612,7 @@
                     up(i, j, h).wait_send()
 
         def returned(cc, h):
-            c = t * per_owner + cc
-            near(c, cc, 2, h).wait_send()
+            near(cc, 2, h).wait_send()
             for j in range(2):
                 @pl.when(inner)
                 def _(j=j):
@@ -549,7 +620,7 @@
 
                 @pl.when(jnp.logical_not(inner))
                 def _(j=j):
-                    near(c, cc, j, h).wait_send()
+                    near(cc, j, h).wait_send()
 
         @pl.loop(0, n - 2)
         def _(i):
@@ -591,6 +662,7 @@
     experts, chunk, width = w_gate.shape
     chunks = ng * nz
     per_owner = chunks // nt
+    cap = 3 * rows // experts
     bf, f32 = jnp.bfloat16, jnp.float32
     dma = pltpu.SemaphoreType.DMA
     full = pltpu.VMEM((d, width), bf)
@@ -603,9 +675,11 @@
         out_specs=(vmem,) * 4,
         scratch_shapes=[
             pltpu.VMEM((nz, rows, d), bf),
-            pltpu.VMEM((nz, rows, width), bf),
-            pltpu.VMEM((chunks, nz, rows, chunk), bf),
-            pltpu.VMEM((chunks // 2, nz, rows, chunk), bf),
+            pltpu.VMEM((nz, cap, d), bf),
+            pltpu.VMEM((nz, cap, width), bf),
+            pltpu.VMEM((chunks, nz, cap, chunk), bf),
+            pltpu.VMEM((chunks // 2, nz, cap, chunk), bf),
+            pltpu.VMEM((per_owner, nz, cap, chunk), bf),
             pltpu.VMEM((per_owner, nz, rows, chunk), bf),
             pltpu.VMEM((2, nz, chunk, width), bf),
             pltpu.VMEM((rows, d), bf),
@@ -613,8 +687,11 @@
             pltpu.VMEM((2, per_owner, rows, chunk), bf),
             pltpu.VMEM((nz, 1, rows), f32),
             pltpu.VMEM((nz, 1, rows), f32),
-            pltpu.VMEM((nz, rows, 128), f32),
+            pltpu.VMEM((nz, cap, 128), f32),
             pltpu.VMEM((chunk, 128), f32),
+            pltpu.VMEM((rows, rows), bf),
+            pltpu.VMEM((cap, rows), bf),
+            pltpu.VMEM((nz, rows, cap), bf),
             dma((4,)),
             dma((2, nz)), dma((nz,)),
             dma((3, nz)), dma((3, nz)),

time: 204 us -> 200 us (0.980)
  Pallas kernels: 202 us -> 198 us
    pallas_call x1, Pallas kernels: 197 us -> 193 us  [fused(): pl.pallas_call(functools.partial(kernel, ng, nz, nt), out_shape=(full, fu...]
where the time goes in v4:
time: 200 us; the launch traced here: 199 us
  Pallas kernels  198 us (99%)
    pallas_call x1, Pallas kernels, fused(): pl.pallas_call(functools.partial(kernel, ng, nz, nt), out_shape=(full, fu...  193 us
    pallas_call x1, Pallas kernels, fused(): pl.pallas_call(store, out_shape=(whole, whole, whole, jax.ShapeDtypeStruc...  4.73 us

profile of v4, /device:TPU:12, one launch (start us, length us, event | category | flops | bytes accessed | tf_op | source)
XLA Modules:
  0.0 198.7 jit_solution(1936230351614237142)
XLA Ops:
  0.6 193.4 %shard_map.102 = (bf16[2048,1024]{1,0:T(8,128)(2,1)S(1)}, bf16[2048,1024]{1,0:T(8,128)(2,1)S(1)}, bf16[2048,1024]{1,0:T(8,128)(2,1)S(1)}, bf16[512,512]{1,0:T(8,128)(2,1)S(1)}) custom-call(bf16[512,2048]{1,0:T(8,128)(2,1)} %tok_in.1, s32[2,512]{1,0:T(2,128)} %bitcast.3, f32[2,512]{1,0:T(2,128)} %bitcast.4, f32[1,256]{1,0:T(1,128)} %bitcast.5, ...), custom_call_target="tpu_custom_call" | custom-call | tf_op jit(solution)/shard_map/pallas_call | solution.py:671
  194.0 4.7 %shard_map.103 = (bf16[1,2048,1024]{2,1,0:T(8,128)(2,1)}, bf16[1,2048,1024]{2,1,0:T(8,128)(2,1)}, bf16[1,2048,1024]{2,1,0:T(8,128)(2,1)}, bf16[512,512]{1,0:T(8,128)(2,1)}) custom-call(bf16[2048,1024]{1,0:T(8,128)(2,1)S(1)} %get-tuple-element.8.gate, bf16[2048,1024]{1,0:T(8,128)(2,1)S(1)} %get-tuple-element.9.upper, ...), custom_call_target="tpu_custom_call" | custom-call | tf_op jit(solution)/shard_map/pallas_call | solution.py:711

commit v5 on v4

--- a/solution.py
+++ b/solution.py
@@ -362,9 +362,11 @@
         def _():
             z_down_side()
 
-        @pl.when(jnp.logical_and(jnp.logical_not(inner), i == nb * nz))
-        def _():
-            z_down_cross()
+        @pl.when(i == nb * nz)
+        def _():
+            @pl.when(ends)
+            def _():
+                z_down_cross()
             zd_take(k_near)
 
         @pl.when(s == 0)
@@ -415,6 +417,8 @@
         for m in ms:
             ref = dpiece(m, 1 - g, frm(k))
             rdma(ref, ref, xs.at[m, nb, k], xr.at[m, nb, k], {"gr": 1 - g}).wait_recv()
+
+    n = chunks
 
     def stage_a(i):
         k, other, c, owner, par, yo, cc = chunk_of(i)
@@ -494,8 +498,12 @@
                     @pl.when(jnp.logical_not(inner))
                     def _(j=j):
                         near(cc, j, h).start()
+                elif j == 2 and h == 1:
+                    near(cc, j, h).start()
                 elif j == 2:
-                    near(cc, j, h).start()
+                    @pl.when(jnp.logical_or(inner, i < n - 4))
+                    def _(j=j):
+                        near(cc, j, h).start()
 
     def cross_phase(cc, h=None):
         for j in range(2):
@@ -504,30 +512,31 @@
             add(full.at[cc, order[j]], h, ref)
             cross(cc, j, h).start()
 
-    n = chunks
     early = jnp.logical_and(inner, side == core)
     late = jnp.logical_and(inner, side != core)
     cc_far = lax.rem(frm(k_far), 2)
 
-    @pl.when(inner)
-    def _():
-        zd_take(k_near)
-
     @pl.loop(0, n - 2)
     def _(i):
-        @pl.when(i == 2)
+        @pl.when(i == 3)
         def _():
             zd_take(k_far, (0,))
 
         @pl.when(i == 4)
         def _():
             zd_take(k_far, (1,))
+
+        @pl.when(i == 5)
+        def _():
             pl.loop(0, 2)(stage_c)
+
+        @pl.when(jnp.logical_or(jnp.logical_and(ends, i == 4), jnp.logical_and(inner, i == 5)))
+        def _():
+            zd_take(k_mid, (0,))
 
         stage_a(i)
         stage_b(i)
 
-    zd_take(k_mid, (0,))
     pl.loop(2, 4)(stage_c)
 
     def last(h):
@@ -537,18 +546,25 @@
         def _(i):
             stage_b(i, h)
 
+    @pl.when(ends)
+    def _():
+        zd_take(k_mid, (1,))
     last(0)
-    zd_take(k_mid, (1,))
+
+    @pl.when(inner)
+    def _():
+        zd_take(k_mid, (1,))
 
     @pl.when(early)
     def _():
         pl.loop(0, per_owner)(cross_phase)
     pl.loop(n - 4, n - 2)(stage_c)
 
+    last(1)
+
     @pl.when(late)
     def _():
         cross_phase(cc_far)
-    last(1)
     for h in range(2):
         @pl.loop(n - 2, n)
         def _(i, h=h):
@@ -557,6 +573,11 @@
         @pl.when(late)
         def _(h=h):
             cross_phase(1 - cc_far, h)
+
+    @pl.when(jnp.logical_and(ends, side != core))
+    def _():
+        near(cc_far, 2, None).start()
+        near(1 - cc_far, 2, 0).start()
 
     def final():
         for cc in range(per_owner):

time: 200 us -> 199 us (level)
  Pallas kernels: 198 us -> 196 us
    pallas_call x1, Pallas kernels: 193 us -> 191 us  [fused(): pl.pallas_call(functools.partial(kernel, ng, nz, nt), out_shape=(full, fu...]
where the time goes in v5:
time: 199 us; the launch traced here: 197 us
  Pallas kernels  196 us (98%)
    pallas_call x1, Pallas kernels, fused(): pl.pallas_call(functools.partial(kernel, ng, nz, nt), out_shape=(full, fu...  191 us
    pallas_call x1, Pallas kernels, fused(): pl.pallas_call(store, out_shape=(whole, whole, whole, jax.ShapeDtypeStruc...  4.73 us

profile of v5, /device:TPU:12, one launch (start us, length us, event | category | flops | bytes accessed | tf_op | source)
XLA Modules:
  0.0 196.6 jit_solution(11766626043798709978)
XLA Ops:
  0.6 191.2 %shard_map.102 = (bf16[2048,1024]{1,0:T(8,128)(2,1)S(1)}, bf16[2048,1024]{1,0:T(8,128)(2,1)S(1)}, bf16[2048,1024]{1,0:T(8,128)(2,1)S(1)}, bf16[512,512]{1,0:T(8,128)(2,1)S(1)}) custom-call(bf16[512,2048]{1,0:T(8,128)(2,1)} %tok_in.1, s32[2,512]{1,0:T(2,128)} %bitcast.3, f32[2,512]{1,0:T(2,128)} %bitcast.4, f32[1,256]{1,0:T(1,128)} %bitcast.5, ...), custom_call_target="tpu_custom_call" | custom-call | tf_op jit(solution)/shard_map/pallas_call | solution.py:692
  191.9 4.7 %shard_map.103 = (bf16[1,2048,1024]{2,1,0:T(8,128)(2,1)}, bf16[1,2048,1024]{2,1,0:T(8,128)(2,1)}, bf16[1,2048,1024]{2,1,0:T(8,128)(2,1)}, bf16[512,512]{1,0:T(8,128)(2,1)}) custom-call(bf16[2048,1024]{1,0:T(8,128)(2,1)S(1)} %get-tuple-element.8.gate, bf16[2048,1024]{1,0:T(8,128)(2,1)S(1)} %get-tuple-element.9.upper, ...), custom_call_target="tpu_custom_call" | custom-call | tf_op jit(solution)/shard_map/pallas_call | solution.py:732

commit v6 on v5

--- a/solution.py
+++ b/solution.py
@@ -362,11 +362,12 @@
         def _():
             z_down_side()
 
+        @pl.when(jnp.logical_and(ends, i == nb * nz - 3))
+        def _():
+            z_down_cross()
+
         @pl.when(i == nb * nz)
         def _():
-            @pl.when(ends)
-            def _():
-                z_down_cross()
             zd_take(k_near)
 
         @pl.when(s == 0)
@@ -530,13 +531,16 @@
         def _():
             pl.loop(0, 2)(stage_c)
 
-        @pl.when(jnp.logical_or(jnp.logical_and(ends, i == 4), jnp.logical_and(inner, i == 5)))
+        @pl.when(jnp.logical_and(ends, i == 4))
         def _():
             zd_take(k_mid, (0,))
 
         stage_a(i)
         stage_b(i)
 
+    @pl.when(inner)
+    def _():
+        zd_take(k_mid, (0,))
     pl.loop(2, 4)(stage_c)
 
     def last(h):

time: 199 us -> 199 us (level)
  no operation moved by 1% of the time
where the time goes in v6:
time: 199 us; the launch traced here: 197 us
  Pallas kernels  196 us (98%)
    pallas_call x1, Pallas kernels, fused(): pl.pallas_call(functools.partial(kernel, ng, nz, nt), out_shape=(full, fu...  191 us
    pallas_call x1, Pallas kernels, fused(): pl.pallas_call(store, out_shape=(whole, whole, whole, jax.ShapeDtypeStruc...  4.73 us

profile of v6, /device:TPU:12, one launch (start us, length us, event | category | flops | bytes accessed | tf_op | source)
XLA Modules:
  0.0 196.7 jit_solution(16189350475417107656)
XLA Ops:
  0.6 191.3 %shard_map.102 = (bf16[2048,1024]{1,0:T(8,128)(2,1)S(1)}, bf16[2048,1024]{1,0:T(8,128)(2,1)S(1)}, bf16[2048,1024]{1,0:T(8,128)(2,1)S(1)}, bf16[512,512]{1,0:T(8,128)(2,1)S(1)}) custom-call(bf16[512,2048]{1,0:T(8,128)(2,1)} %tok_in.1, s32[2,512]{1,0:T(2,128)} %bitcast.3, f32[2,512]{1,0:T(2,128)} %bitcast.4, f32[1,256]{1,0:T(1,128)} %bitcast.5, ...), custom_call_target="tpu_custom_call" | custom-call | tf_op jit(solution)/shard_map/pallas_call | solution.py:696
  191.9 4.7 %shard_map.103 = (bf16[1,2048,1024]{2,1,0:T(8,128)(2,1)}, bf16[1,2048,1024]{2,1,0:T(8,128)(2,1)}, bf16[1,2048,1024]{2,1,0:T(8,128)(2,1)}, bf16[512,512]{1,0:T(8,128)(2,1)}) custom-call(bf16[2048,1024]{1,0:T(8,128)(2,1)S(1)} %get-tuple-element.8.gate, bf16[2048,1024]{1,0:T(8,128)(2,1)S(1)} %get-tuple-element.9.upper, ...), custom_call_target="tpu_custom_call" | custom-call | tf_op jit(solution)/shard_map/pallas_call | solution.py:736
